TPU v7x, 32 devices: a whole 2x2x4 slice. The times are simulated.
32 devices in a mesh: sp: 16 (over z, y, x), tp: 2 (over core).
Axes of the slice: x: 2, y: 2, z: 4, core: 2. Of those that a mesh axis runs over, the one named last changes fastest.
Arguments:
- hidden_in: bfloat16 [8192, 2048], P('sp'), may hold values from -64 to 64
- pre_gain: float32 [2048], replicated, may hold values from 0.1 to 1.9
- query_proj: bfloat16 [2048, 2048], P(None, 'tp'), may hold values from -2 to 2
- key_proj: bfloat16 [2048, 2048], P('sp', 'tp'), may hold values from -2 to 2
- value_proj: bfloat16 [2048, 2048], P('sp', 'tp'), may hold values from -0.125 to 0.125
- out_proj: bfloat16 [2048, 2048], P('tp'), may hold values from -0.125 to 0.125
- post_gain: float32 [2048], replicated, may hold values from 0.1 to 1.9
Outputs:
- layer_out: bfloat16 [8192, 2048], P(('sp', 'tp'))
- log_weight: float32 [32, 8192], P('tp', 'sp')
All inputs are finite; a program needn't handle non-finite values.
Results may differ from a plain program's by a relative error of at most 0.018.
The roundings to bfloat16 on the way count: a program that leaves them out, or rounds other values in their place, can miss the bound.
Values may be sent and summed in bfloat16 or wider, within the bound.
A program may use at most 128 MiB of HBM per device.

v0:
```python
import jax
import jax.numpy as jnp
from jax import lax
from jax.sharding import PartitionSpec as P

HEAD_DIM = 64
SPAN = 128


EPS = 1e-06
ROPE_BASE = 10000.0
DILATIONS = (1, 4, 16)


def passed_along(value, axis, steps):
    count = lax.axis_size(axis)
    first, last = (max(0, -steps), min(count, count - steps))
    return lax.ppermute(value, axis, [(source, source + steps) for source in range(first, last)])


def rotate(vectors, positions):
    half_dim = vectors.shape[-1] // 2
    frequency = ROPE_BASE ** (-(jnp.arange(half_dim, dtype=jnp.float32) * 2.0 / vectors.shape[-1]))
    angles = positions[:, None] * frequency[None, :]
    cos_part = jnp.cos(angles)[:, None, :]
    sin_part = jnp.sin(angles)[:, None, :]
    front_half = vectors[..., :half_dim]
    back_half = vectors[..., half_dim:]
    return jnp.concatenate(
        [
            front_half * cos_part - back_half * sin_part,
            back_half * cos_part + front_half * sin_part,
        ],
        axis=-1,
    )


def rms_scale(matrix, gain):
    return matrix * lax.rsqrt(jnp.mean(matrix * matrix, axis=-1, keepdims=True) + EPS) * gain


def window_group(queries, buffer, dilation, offset):
    local_rows, head_count, head_depth = queries.shape
    reach_rows = dilation * SPAN
    start_row = buffer.shape[1] - local_rows - reach_rows
    key_rows = buffer[0, start_row:]
    value_rows = buffer[1, start_row:]
    res_len = local_rows // dilation
    block_len = min(SPAN, res_len)
    blocks = res_len // block_len
    query_blocks = queries.reshape(blocks, block_len, dilation, head_count, head_depth)
    key_res = key_rows.reshape(-1, dilation, head_count, head_depth)
    value_res = value_rows.reshape(-1, dilation, head_count, head_depth)
    width_keys = block_len + SPAN
    key_sets = jnp.stack(
        [
            key_res[block_idx * block_len : block_idx * block_len + width_keys]
            for block_idx in range(blocks)
        ]
    )
    value_sets = jnp.stack(
        [
            value_res[block_idx * block_len : block_idx * block_len + width_keys]
            for block_idx in range(blocks)
        ]
    )
    scores = jnp.einsum(
        "bqrhe,bkrhe->brhqk", query_blocks, key_sets, preferred_element_type=jnp.float32
    ) * head_depth ** (-0.5)
    query_idx = jnp.arange(block_len, dtype=jnp.int32)[:, None]
    key_idx = jnp.arange(width_keys, dtype=jnp.int32)[None, :]
    distance = query_idx + SPAN - key_idx
    in_band = (distance >= 0) & (distance <= SPAN)
    key_pos = (
        (
            jnp.arange(blocks, dtype=jnp.int32)[:, None, None, None, None] * block_len
            + jnp.arange(width_keys, dtype=jnp.int32)[None, None, None, None, :]
        )
        * dilation
        + jnp.arange(dilation, dtype=jnp.int32)[None, :, None, None, None]
        + (offset - reach_rows)
    )
    valid = in_band[None, None, None] & (key_pos >= 0)
    scores = jnp.where(valid, scores, -jnp.inf)
    row_max = jnp.max(scores, axis=-1, keepdims=True)
    exp_scores = jnp.exp(scores - row_max)
    denominator = jnp.sum(exp_scores, axis=-1, keepdims=True)
    levels = (row_max + jnp.log(denominator))[..., 0]
    shares = (exp_scores / denominator).astype(jnp.bfloat16)
    outcome = jnp.einsum(
        "brhqk,bkrhe->bqrhe", shares, value_sets, preferred_element_type=jnp.float32
    )
    outcome = outcome.reshape(local_rows, head_count, head_depth)
    levels = levels.transpose(2, 0, 3, 1).reshape(head_count, local_rows)
    return (outcome, levels)


def blend(group_outs, group_levels):
    levels = jnp.stack(group_levels)
    row_max = jnp.max(levels, axis=0)
    log_weight = row_max + jnp.log(jnp.sum(jnp.exp(levels - row_max[None]), axis=0))
    shares = jnp.exp(levels - log_weight[None])
    blended = jnp.sum(shares.transpose(0, 2, 1)[..., None] * jnp.stack(group_outs), axis=0)
    return (blended, log_weight)


def body(hidden_in, pre_gain, query_proj, key_proj, value_proj, out_proj, post_gain):
    local_rows = hidden_in.shape[0]
    local_width = query_proj.shape[1]
    head_count = local_width // HEAD_DIM
    normed = rms_scale(hidden_in.astype(jnp.float32), pre_gain).astype(jnp.bfloat16)
    offset = lax.axis_index("sp") * local_rows
    positions = (offset + jnp.arange(local_rows, dtype=jnp.int32)).astype(jnp.float32)
    queries = rotate(
        jnp.dot(normed, query_proj, preferred_element_type=jnp.float32).reshape(
            local_rows, head_count, HEAD_DIM
        ),
        positions,
    ).astype(jnp.bfloat16)
    pieces = (
        lax.all_gather(key_proj, "sp", axis=0, tiled=True),
        lax.all_gather(value_proj, "sp", axis=0, tiled=True),
    )
    key_sum = jnp.dot(normed, pieces[0], preferred_element_type=jnp.float32)
    value_sum = jnp.dot(normed, pieces[1], preferred_element_type=jnp.float32)
    key_rows = (
        rotate(key_sum.reshape(local_rows, head_count, HEAD_DIM), positions)
        .astype(jnp.bfloat16)
        .reshape(local_rows, local_width)
    )
    key_value = jnp.stack([key_rows, value_sum.astype(jnp.bfloat16)])
    behind = -(-(16 * SPAN) // local_rows)
    pieces = [passed_along(key_value, "sp", distance) for distance in range(behind, 0, -1)]
    buffer = jnp.concatenate(pieces + [key_value], axis=1)
    buffer = buffer.reshape(2, buffer.shape[1], head_count, HEAD_DIM)
    group_outs = []
    group_levels = []
    for dilation in DILATIONS:
        outcome, levels = window_group(queries, buffer, dilation, offset)
        group_outs.append(outcome)
        group_levels.append(levels)
    blended, log_weight = blend(group_outs, group_levels)
    attended = blended.astype(jnp.bfloat16).reshape(local_rows, local_width)
    summed = lax.psum_scatter(
        jnp.dot(attended, out_proj, preferred_element_type=jnp.float32).astype(jnp.bfloat16),
        "tp",
        scatter_dimension=0,
        tiled=True,
    ).astype(jnp.float32)
    layer_out = rms_scale(summed, post_gain).astype(jnp.bfloat16)
    return (layer_out, log_weight)


def solution(mesh):
    placed = (P("sp", None), P(), P(None, "tp"), P("sp", "tp"), P("sp", "tp"), P("tp", None), P())
    return jax.shard_map(
        body,
        mesh=mesh,
        in_specs=placed,
        out_specs=(P(("sp", "tp"), None), P("tp", "sp")),
        check_vma=False,
    )
```

profile of v0, /device:TPU:0, one launch (start us, length us, event | category | flops | bytes accessed | tf_op | source)
XLA Modules:
  0.0 570.0 jit_solution(712279927892896945)
XLA Ops:
  7.2 0.7 all-gather.3.cloned.1.call-update
  7.9 0.7 all-gather.5.cloned.1.call-update
  8.7 2.1 fusion.11
  11.2 5.3 fusion.78
  16.5 72.6 %all-gather.3.cloned.1.call-done = bf16[2048,1024]{1,0:T(8,128)(2,1)} async-done(((bf16[128,1024]{1,0:T(8,128)(2,1)}), bf16[2048,1024]{1,0:T(8,128)(2,1)}) %all-gather.3.cloned.1.call-update) | async-done | bytes 4194320 | tf_op jit(solution)/shard_map/all_gather | solution.py:121
  89.1 5.3 fusion.76
  94.4 1.6 subtract_convert_fusion.1
  96.6 69.4 %all-gather.5.cloned.1.call-done = bf16[2048,1024]{1,0:T(8,128)(2,1)} async-done(((bf16[128,1024]{1,0:T(8,128)(2,1)}), bf16[2048,1024]{1,0:T(8,128)(2,1)}) %all-gather.5.cloned.1.call-update) | async-done | bytes 4194320 | tf_op jit(solution)/shard_map/all_gather | solution.py:122
  166.1 5.2 fusion.51
  171.3 1.0 copy-done.8
  172.3 1.5 pad_maximum_fusion
  173.8 4.7 collective-permute-start
  178.5 4.8 collective-permute-start.1
  183.3 3.8 collective-permute-start.2
  187.1 2.8 collective-permute-start.3
  190.3 2.9 copy.102
  193.2 2.8 copy.104
  196.1 3.7 copy.101
  199.8 3.9 copy.103
  203.7 4.4 copy.110
  208.1 2.7 copy.111
  210.8 0.9 copy_bitcast_fusion.1
  211.7 0.9 copy_bitcast_fusion
  212.7 8.5 %collective-permute-done = bf16[2,512,1024]{2,1,0:T(8,128)(2,1)} collective-permute-done((bf16[2,512,1024]{2,1,0:T(8,128)(2,1)}, bf16[2,512,1024]{2,1,0:T(8,128)(2,1)}, u32[]{:S(2)}, u32[]{:S(2)}) %collective-permute-start) | collective-permute-done | bytes 2097184 | tf_op jit(solution)/shard_map/ppermute | solution.py:18
  221.2 3.2 constant_dynamic-update-slice_fusion.4
  224.3 3.9 collective-permute-done.1
  228.2 3.1 constant_dynamic-update-slice_fusion.3
  231.3 43.3 %collective-permute-done.2 = bf16[2,512,1024]{2,1,0:T(8,128)(2,1)} collective-permute-done((bf16[2,512,1024]{2,1,0:T(8,128)(2,1)}, bf16[2,512,1024]{2,1,0:T(8,128)(2,1)}, u32[]{:S(2)}, u32[]{:S(2)}) %collective-permute-start.2) | collective-permute-done | bytes 2097184 | tf_op jit(solution)/shard_map/ppermute | solution.py:18
  274.6 3.1 constant_dynamic-update-slice_fusion.2
  277.7 3.1 constant_dynamic-update-slice_fusion.1
  280.8 1.6 constant_dynamic-update-slice_fusion
  282.4 13.8 %copy.99 = bf16[2,2560,1024]{1,2,0:T(8,128)(2,1)} copy(bf16[2,2560,1024]{2,1,0:T(8,128)(2,1)} %constant_dynamic-update-slice_fusion) | data formatting | bytes 20971520 | tf_op jit(solution)/shard_map/concatenate | solution.py:134
  296.2 9.2 %fusion.81 = (bf16[1,2560,1024]{2,1,0:T(8,128)(2,1)}, bf16[1,2560,1024]{2,1,0:T(8,128)(2,1)}) fusion(bf16[2,2560,1024]{2,1,0:T(8,128)(2,1)} %constant_dynamic-update-slice_fusion), kind=kLoop, calls=%fused_computation.140 | loop fusion | bytes 20971520 | tf_op jit(solution)/shard_map/slice | solution.py:46
  305.4 4.4 slice_bitcast_fusion.3
  309.8 5.0 fusion.80
  314.8 15.0 %reshape.505 = bf16[160,16,16,64]{3,2,1,0:T(8,128)(2,1)} reshape(bf16[1,2560,1024]{2,1,0:T(8,128)(2,1)} %get-tuple-element.14) | data formatting | bytes 10485760 | tf_op jit(solution)/shard_map/reshape.43
  329.8 18.8 %fusion.7 = (f32[16,16,32]{2,1,0:T(8,128)S(1)}, f32[16,16,32,160]{3,2,1,0:T(8,128)}) fusion(pred[16,32,160]{2,1,0:T(8,128)(4,1)S(1)} %broadcast_and_fusion, bf16[160,16,16,64]{3,2,1,0:T(8,128)(2,1)} %reshape.505, bf16[32,16,16,32]{3,0,2,1:T(8,128)(2,1)} %copy.111, bf16[32,16,16,32]{3,0,2,1:T(8,128)(2,1)S(1)} %copy-done), kind=kOutput, calls=%fused_computation.17 | convolution fusion | flops 173793280 | bytes 11649024 | tf_op jit(solution)/shard_map/bqrhe,bkrhe->brhqk/dot_general | solution.py:67
  348.6 5.2 fusion.10
  353.8 0.7 add_bitcast_fusion
  354.5 1.0 copy.113
  355.5 0.8 stack_reshape.34
  356.3 0.8 stack_reshape.30
  357.0 4.9 copy.105
  362.0 8.3 %fusion.6 = (f32[4,16,128]{2,1,0:T(8,128)S(1)}, f32[4,16,128,256]{3,2,1,0:T(8,128)S(1)}) fusion(pred[4,128,256]{2,1,0:T(8,128)(4,1)S(1)} %get-tuple-element.23, bf16[256,4,16,64]{3,2,1,0:T(8,128)(2,1)} %bitcast.111, bf16[128,4,16,32]{0,3,2,1:T(8,128)(2,1)S(1)} %copy-done.10, bf16[128,4,16,32]{0,3,2,1:T(8,128)(2,1)} %copy.103), kind=kOutput, calls=%fused_computation.16 | convolution fusion | flops 276815872 | bytes 11698176 | tf_op jit(solution)/shard_map/bqrhe,bkrhe->brhqk/dot_general | solution.py:67
  370.4 2.4 fusion.5
  372.8 0.8 copy-done.3
  373.6 7.0 %fusion.8 = (f32[4,16,128]{2,1,0:T(8,128)S(1)}, f32[4,16,128]{2,1,0:T(8,128)S(1)}) fusion(f32[4,16,128,256]{3,2,1,0:T(8,128)S(1)} %get-tuple-element.31, f32[4,16,128]{2,1,0:T(8,128)S(1)} %get-tuple-element.30, pred[4,128,256]{2,1,0:T(8,128)(4,1)S(1)} %get-tuple-element.22, f32[4,16,128]{2,1,0:T(8,128)S(1)} %get-tuple-element.28, ...), kind=kLoop, calls=%fused_computation.18 | loop fusion | flops 16760832 | bytes 17170432 | tf_op jit(solution)/shard_map/reduce_sum | solution.py:87
  380.7 0.6 copy.116
  382.0 5.1 copy.121
  387.0 0.6 add_bitcast_fusion.1
  387.7 9.0 %fusion.48 = f32[1,128,4,16,64]{1,4,3,2,0:T(8,128)S(1)} fusion(f32[4,16,128,256]{3,2,1,0:T(8,128)} %copy-done.3, f32[4,16,128]{2,1,0:T(8,128)} %copy-done.28, f32[4,16,128]{2,1,0:T(8,128)} %copy-done.25, pred[4,128,256]{2,1,0:T(8,128)(4,1)S(1)} %get-tuple-element.23, bf16[256,4,16,64]{3,2,1,0:T(8,128)(2,1)} %bitcast.110), kind=kOutput, calls=%fused_computation.64 | convolution fusion | flops 278921216 | bytes 12779520 | tf_op jit(solution)/shard_map/brhqk,bkrhe->bqrhe/dot_general | solution.py:90
  396.9 2.7 fusion.47
  399.6 2.7 copy.120
  403.1 4.5 copy.123
  407.6 5.8 %copy.126 = f32[1,512,16,64]{1,0,3,2:T(1,128)S(1)} copy(f32[1,512,16,64]{3,2,1,0:T(8,128)} %bitcast.107) | data formatting | bytes 4194304 | tf_op jit(solution)/shard_map/stack;reshape | solution.py:103
  413.4 14.4 %reshape.508 = bf16[160,16,16,64]{3,2,1,0:T(8,128)(2,1)} reshape(bf16[1,2560,1024]{2,1,0:T(8,128)(2,1)} %get-tuple-element.15) | data formatting | bytes 10485760 | tf_op jit(solution)/shard_map/reshape.68
  427.9 15.4 %fusion.25 = f32[1,32,16,16,64]{4,1,3,2,0:T(8,128)S(1)} fusion(bf16[160,16,16,64]{3,2,1,0:T(8,128)(2,1)} %reshape.508, f32[16,16,32,160]{3,2,1,0:T(8,128)} %get-tuple-element.27, f32[16,16,32]{2,1,0:T(8,128)S(1)} %fusion.10, f32[16,16,32]{2,1,0:T(8,128)S(1)} %get-tuple-element.26, pred[16,32,160]{2,1,0:T(8,128)(4,1)S(1)} %broadcast_and_fusion), kind=kOutput, calls=%fused_computation.40 | convolution fusion | flops 174325760 | bytes 12730368 | tf_op jit(solution)/shard_map/brhqk,bkrhe->bqrhe/dot_general | solution.py:90
  443.2 4.5 copy.125
  447.7 6.8 %copy.127 = f32[1,512,16,64]{1,0,3,2:T(1,128)} copy(f32[1,512,16,64]{3,2,1,0:T(8,128)} %bitcast.108) | data formatting | bytes 4194304 | tf_op jit(solution)/shard_map/stack;reshape | solution.py:103
  454.5 11.5 %fusion.4 = bf16[512,16,64]{0,2,1:T(8,128)(2,1)S(1)} fusion(f32[1,512,16,64]{1,0,3,2:T(1,128)} %copy.127, f32[1,512,16,64]{1,0,3,2:T(1,128)S(1)} %copy.126, f32[1,512,16,64]{1,0,3,2:T(1,128)} %bitcast.109, f32[3,512,16]{1,0,2:T(4,128)S(1)} %exponential_bitcast_fusion), kind=kLoop, calls=%fused_computation.5 | loop fusion | flops 5767168 | bytes 7438336 | tf_op jit(solution)/shard_map/reduce_sum | solution.py:103
  466.1 3.8 convolution_convert_fusion
  469.9 89.2 %reduce-scatter.2.cloned.1.call-done = bf16[256,2048]{1,0:T(8,128)(2,1)} async-done(((bf16[512,2048]{1,0:T(8,128)(2,1)}), bf16[256,2048]{1,0:T(8,128)(2,1)}) %reduce-scatter.2.cloned.1.call-update) | async-done | bytes 1048592 | tf_op jit(solution)/shard_map/reduce_scatter | solution.py:144
  559.0 1.5 fusion.28
  560.5 2.5 fusion.30
  (103 shorter events, 3.0 us)
Async XLA Ops:
  7.2 81.9 %all-gather.3.cloned.1.call-start = ((), (), s32[]{:S(2)}) async-start(), calls=%async_computation.1 | async-start | bytes 4456448 | tf_op jit(solution)/shard_map/all_gather | solution.py:121
  7.9 158.2 %all-gather.5.cloned.1.call-start = ((), (), s32[]{:S(2)}) async-start(), calls=%async_computation.2 | async-start | bytes 4456448 | tf_op jit(solution)/shard_map/all_gather | solution.py:122
  8.6 550.4 %reduce-scatter.2.cloned.1.call-start = ((), (), s32[]{:S(2)}) async-start(), calls=%async_computation.3 | async-start | bytes 3145728 | tf_op jit(solution)/shard_map/reduce_scatter | solution.py:144
  11.2 77.9 %copy-start.35 = (f32[2048]{0:T(1024)S(1)}, f32[2048]{0:T(1024)}, u32[]{:S(2)}) copy-start(f32[2048]{0:T(1024)} %param.8) | copy-start | bytes 24580
  171.3 1.0 copy-start.8
  173.8 47.4 %collective-permute-start = (bf16[2,512,1024]{2,1,0:T(8,128)(2,1)}, bf16[2,512,1024]{2,1,0:T(8,128)(2,1)}, u32[]{:S(2)}, u32[]{:S(2)}) collective-permute-start(bf16[2,512,1024]{2,1,0:T(8,128)(2,1)} %pad_maximum_fusion), channel_id=1, source_target_pairs={{0,8},{2,10},{4,12},{6,14},{8,16},{10,18},{12,20},{14,22},{16,24},... | collective-permute-start | bytes 6291464 | tf_op jit(solution)/shard_map/ppermute | solution.py:18
  178.5 49.7 %collective-permute-start.1 = (bf16[2,512,1024]{2,1,0:T(8,128)(2,1)}, bf16[2,512,1024]{2,1,0:T(8,128)(2,1)}, u32[]{:S(2)}, u32[]{:S(2)}) collective-permute-start(bf16[2,512,1024]{2,1,0:T(8,128)(2,1)} %pad_maximum_fusion), channel_id=1, source_target_pairs={{0,6},{2,8},{4,10},{6,12},{8,14},{10,16},{12,18},{14,20},{16,22},{... | collective-permute-start | bytes 6291464 | tf_op jit(solution)/shard_map/ppermute | solution.py:18
  183.3 91.3 %collective-permute-start.2 = (bf16[2,512,1024]{2,1,0:T(8,128)(2,1)}, bf16[2,512,1024]{2,1,0:T(8,128)(2,1)}, u32[]{:S(2)}, u32[]{:S(2)}) collective-permute-start(bf16[2,512,1024]{2,1,0:T(8,128)(2,1)} %pad_maximum_fusion), channel_id=1, source_target_pairs={{0,4},{2,6},{4,8},{6,10},{8,12},{10,14},{12,16},{14,18},{16,20},{1... | collective-permute-start | bytes 6291464 | tf_op jit(solution)/shard_map/ppermute | solution.py:18
  187.1 90.6 %collective-permute-start.3 = (bf16[2,512,1024]{2,1,0:T(8,128)(2,1)}, bf16[2,512,1024]{2,1,0:T(8,128)(2,1)}, u32[]{:S(2)}, u32[]{:S(2)}) collective-permute-start(bf16[2,512,1024]{2,1,0:T(8,128)(2,1)} %pad_maximum_fusion), channel_id=1, source_target_pairs={{0,2},{2,4},{4,6},{6,8},{8,10},{10,12},{12,14},{14,16},{16,18},{18... | collective-permute-start | bytes 6291464 | tf_op jit(solution)/shard_map/ppermute | solution.py:18
  203.7 7.1 %copy-start.7 = (bf16[512,16,32]{0,2,1:T(8,128)(2,1)S(1)}, bf16[512,16,32]{0,2,1:T(8,128)(2,1)}, u32[]{:S(2)}) copy-start(bf16[512,16,32]{0,2,1:T(8,128)(2,1)} %get-tuple-element.16) | copy-start | bytes 1572868
  203.7 8.1 %copy-start.6 = (bf16[512,16,32]{0,2,1:T(8,128)(2,1)S(1)}, bf16[512,16,32]{0,2,1:T(8,128)(2,1)}, u32[]{:S(2)}) copy-start(bf16[512,16,32]{0,2,1:T(8,128)(2,1)} %get-tuple-element.17) | copy-start | bytes 1572868
  231.3 49.5 %copy-start.9 = (bf16[1,512,1024]{2,1,0:T(8,128)(2,1)S(1)}, bf16[1,512,1024]{2,1,0:T(8,128)(2,1)}, u32[]{:S(2)}) copy-start(bf16[1,512,1024]{2,1,0:T(8,128)(2,1)} %copy-done.8) | copy-start | bytes 3145732
  314.8 15.0 %copy-start = (bf16[32,16,16,32]{3,0,2,1:T(8,128)(2,1)S(1)}, bf16[32,16,16,32]{3,0,2,1:T(8,128)(2,1)}, u32[]{:S(2)}) copy-start(bf16[32,16,16,32]{3,0,2,1:T(8,128)(2,1)} %copy.110) | copy-start | bytes 1572868
  348.6 8.4 %copy-start.5 = (bf16[1,1024,16,64]{1,3,2,0:T(8,128)(2,1)S(1)}, bf16[1,1024,16,64]{1,3,2,0:T(8,128)(2,1)}, u32[]{:S(2)}) copy-start(bf16[1,1024,16,64]{1,3,2,0:T(8,128)(2,1)} %get-tuple-element.13) | copy-start | bytes 6291460
  353.8 8.2 %copy-start.10 = (bf16[128,4,16,32]{0,3,2,1:T(8,128)(2,1)S(1)}, bf16[128,4,16,32]{0,3,2,1:T(8,128)(2,1)}, u32[]{:S(2)}) copy-start(bf16[128,4,16,32]{0,3,2,1:T(8,128)(2,1)} %copy.104) | copy-start | bytes 1572868
  361.9 8.4 %copy-start.15 = (bf16[1,256,1,16,64]{1,4,3,0,2:T(8,128)(2,1)S(1)}, bf16[1,256,1,16,64]{1,4,3,0,2:T(8,128)(2,1)}, u32[]{:S(2)}) copy-start(bf16[1,256,1,16,64]{1,4,3,0,2:T(8,128)(2,1)} %get-tuple-element.8) | copy-start | bytes 1572868
  361.9 8.4 %copy-start.16 = (bf16[1,256,1,16,64]{1,4,3,0,2:T(8,128)(2,1)S(1)}, bf16[1,256,1,16,64]{1,4,3,0,2:T(8,128)(2,1)}, u32[]{:S(2)}) copy-start(bf16[1,256,1,16,64]{1,4,3,0,2:T(8,128)(2,1)} %get-tuple-element.9) | copy-start | bytes 1572868
  361.9 8.4 %copy-start.17 = (bf16[1,256,1,16,64]{1,4,3,0,2:T(8,128)(2,1)S(1)}, bf16[1,256,1,16,64]{1,4,3,0,2:T(8,128)(2,1)}, u32[]{:S(2)}) copy-start(bf16[1,256,1,16,64]{1,4,3,0,2:T(8,128)(2,1)} %get-tuple-element.10) | copy-start | bytes 1572868
  361.9 8.4 %copy-start.18 = (bf16[1,256,1,16,64]{1,4,3,0,2:T(8,128)(2,1)S(1)}, bf16[1,256,1,16,64]{1,4,3,0,2:T(8,128)(2,1)}, u32[]{:S(2)}) copy-start(bf16[1,256,1,16,64]{1,4,3,0,2:T(8,128)(2,1)} %get-tuple-element.11) | copy-start | bytes 1572868
  361.9 8.4 %copy-start.19 = (bf16[4,128,16,32]{1,3,2,0:T(8,128)(2,1)S(1)}, bf16[4,128,16,32]{1,3,2,0:T(8,128)(2,1)}, u32[]{:S(2)}) copy-start(bf16[4,128,16,32]{1,3,2,0:T(8,128)(2,1)} %copy_bitcast_fusion.1) | copy-start | bytes 1572868
  362.0 8.4 %copy-start.20 = (bf16[4,128,16,32]{1,3,2,0:T(8,128)(2,1)S(1)}, bf16[4,128,16,32]{1,3,2,0:T(8,128)(2,1)}, u32[]{:S(2)}) copy-start(bf16[4,128,16,32]{1,3,2,0:T(8,128)(2,1)} %copy_bitcast_fusion) | copy-start | bytes 1572868
  370.3 3.3 copy-start.3
  370.3 16.7 %copy-start.25 = (f32[4,16,128]{2,1,0:T(8,128)}, f32[4,16,128]{2,1,0:T(8,128)S(1)}, u32[]{:S(2)}) copy-start(f32[4,16,128]{2,1,0:T(8,128)S(1)} %get-tuple-element.28) | copy-start | bytes 98308
  372.8 7.8 %copy-start.1 = (f32[4,16,128,256]{3,2,1,0:T(8,128)}, f32[4,16,128,256]{3,2,1,0:T(8,128)S(1)}, u32[]{:S(2)}) copy-start(f32[4,16,128,256]{3,2,1,0:T(8,128)S(1)} %get-tuple-element.31) | copy-start | bytes 25165828
  372.8 7.9 %copy-start.23 = (f32[4,16,128]{2,1,0:T(8,128)}, f32[4,16,128]{2,1,0:T(8,128)S(1)}, u32[]{:S(2)}) copy-start(f32[4,16,128]{2,1,0:T(8,128)S(1)} %get-tuple-element.30) | copy-start | bytes 98308
  373.6 8.3 %copy-start.4 = (bf16[1,1024,16,64]{1,3,2,0:T(8,128)(2,1)S(1)}, bf16[1,1024,16,64]{1,3,2,0:T(8,128)(2,1)}, u32[]{:S(2)}) copy-start(bf16[1,1024,16,64]{1,3,2,0:T(8,128)(2,1)} %get-tuple-element.12) | copy-start | bytes 6291460
  380.7 7.0 %copy-start.26 = (f32[4,16,128]{2,1,0:T(8,128)}, f32[4,16,128]{2,1,0:T(8,128)S(1)}, u32[]{:S(2)}) copy-start(f32[4,16,128]{2,1,0:T(8,128)S(1)} %get-tuple-element.32) | copy-start | bytes 98308
  380.7 7.0 %copy-start.28 = (f32[4,16,128]{2,1,0:T(8,128)}, f32[4,16,128]{2,1,0:T(8,128)S(1)}, u32[]{:S(2)}) copy-start(f32[4,16,128]{2,1,0:T(8,128)S(1)} %get-tuple-element.33) | copy-start | bytes 98308
  387.7 9.1 %copy-start.2 = (f32[4,16,128,256]{3,2,1,0:T(8,128)S(1)}, f32[4,16,128,256]{3,2,1,0:T(8,128)}, u32[]{:S(2)}) copy-start(f32[4,16,128,256]{3,2,1,0:T(8,128)} %copy-done.1) | copy-start | bytes 25165828
  387.7 9.1 %copy-start.11 = (bf16[1,256,1,16,64]{1,4,3,0,2:T(8,128)(2,1)S(1)}, bf16[1,256,1,16,64]{1,4,3,0,2:T(8,128)(2,1)}, u32[]{:S(2)}) copy-start(bf16[1,256,1,16,64]{1,4,3,0,2:T(8,128)(2,1)} %get-tuple-element.4) | copy-start | bytes 1572868
  387.7 9.1 %copy-start.12 = (bf16[1,256,1,16,64]{1,4,3,0,2:T(8,128)(2,1)S(1)}, bf16[1,256,1,16,64]{1,4,3,0,2:T(8,128)(2,1)}, u32[]{:S(2)}) copy-start(bf16[1,256,1,16,64]{1,4,3,0,2:T(8,128)(2,1)} %get-tuple-element.5) | copy-start | bytes 1572868
  387.7 9.1 %copy-start.13 = (bf16[1,256,1,16,64]{1,4,3,0,2:T(8,128)(2,1)S(1)}, bf16[1,256,1,16,64]{1,4,3,0,2:T(8,128)(2,1)}, u32[]{:S(2)}) copy-start(bf16[1,256,1,16,64]{1,4,3,0,2:T(8,128)(2,1)} %get-tuple-element.6) | copy-start | bytes 1572868
  387.7 9.1 %copy-start.14 = (bf16[1,256,1,16,64]{1,4,3,0,2:T(8,128)(2,1)S(1)}, bf16[1,256,1,16,64]{1,4,3,0,2:T(8,128)(2,1)}, u32[]{:S(2)}) copy-start(bf16[1,256,1,16,64]{1,4,3,0,2:T(8,128)(2,1)} %get-tuple-element.7) | copy-start | bytes 1572868
  387.7 9.1 %copy-start.24 = (f32[4,16,128]{2,1,0:T(8,128)S(1)}, f32[4,16,128]{2,1,0:T(8,128)}, u32[]{:S(2)}) copy-start(f32[4,16,128]{2,1,0:T(8,128)} %copy-done.23) | copy-start | bytes 98308
  387.7 9.1 %copy-start.27 = (f32[4,16,128]{2,1,0:T(8,128)S(1)}, f32[4,16,128]{2,1,0:T(8,128)}, u32[]{:S(2)}) copy-start(f32[4,16,128]{2,1,0:T(8,128)} %copy-done.26) | copy-start | bytes 98308
  399.6 2.8 copy-start.29
  399.6 3.1 copy-start.30
  399.6 3.1 copy-start.31
  399.6 3.1 copy-start.21
  399.6 3.1 copy-start.22
  403.0 10.5 %copy-start.32 = (f32[16,512]{1,0:T(8,128)}, f32[16,512]{1,0:T(8,128)S(1)}, u32[]{:S(2)}) copy-start(f32[16,512]{1,0:T(8,128)S(1)} %log_add_fusion) | copy-start | bytes 98308
  454.5 11.5 %copy-start.34 = (bf16[1024,2048]{1,0:T(8,128)(2,1)S(1)}, bf16[1024,2048]{1,0:T(8,128)(2,1)}, u32[]{:S(2)}) copy-start(bf16[1024,2048]{1,0:T(8,128)(2,1)} %param.12) | copy-start | bytes 12582916
  466.0 94.5 %copy-start.33 = (f32[2048]{0:T(1024)S(1)}, f32[2048]{0:T(1024)}, u32[]{:S(2)}) copy-start(f32[2048]{0:T(1024)} %param.13) | copy-start | bytes 24580
Sparse Core Ops, SparseCore 0:
  10.7 78.3 all-gather.2
  91.9 74.1 all-gather.4
  470.0 88.9 reduce-scatter.1
where the time goes:
time: 579 us; the launch traced here: 570 us
  waiting for transfers between devices  288 us (50%)
  local copies, waits for them, and re-layouts  137 us (24%)
  matrix products  76.2 us (13%)
  other arithmetic  37.1 us (6%)
  starting transfers between devices  16.2 us (3%)
  between operations  14.8 us (3%)
    reduce_scatter x1, waiting for transfers between devices, body(): lax.psum_scatter(jnp.dot(attended, out_proj, preferred_element_type=jnp.f...  89.2 us
    all_gather x1, waiting for transfers between devices, body(): lax.all_gather(key_proj, 'sp', axis=0, tiled=True)  72.6 us
    all_gather x1, waiting for transfers between devices, body(): lax.all_gather(value_proj, 'sp', axis=0, tiled=True)  69.4 us
    ppermute x4, waiting for transfers between devices, passed_along(): lax.ppermute(value, axis, [(source, source + steps) for source in range(f...  55.7 us
    another operation x4, local copies, waits for them, and re-layouts  36 us
    dot_general x3, matrix products, window_group(): jnp.einsum('bqrhe,bkrhe->brhqk', query_blocks, key_sets, preferred_elemen...  29.6 us
    dot_general x3, matrix products, window_group(): jnp.einsum('brhqk,bkrhe->bqrhe', shares, value_sets, preferred_element_ty...  27.1 us
    ppermute x4, starting transfers between devices, passed_along(): lax.ppermute(value, axis, [(source, source + steps) for source in range(f...  16.1 us
  transfers between devices with their start and end apart: 7, of which 6 were waited for; matrix products, arithmetic and copies ran while one was open for 8% of the time, Pallas kernels for 0%

commit v1 on v0

v1 whole, which is shorter than its diff:
```python
import functools

import jax
import jax.numpy as jnp
from jax import lax
from jax.experimental import pallas as pl
from jax.experimental.pallas import tpu as pltpu
from jax.sharding import PartitionSpec as P

HEAD_DIM = 64
SPAN = 128
EPS = 1e-06
ROPE_BASE = 10000.0
WIDE = 16
LANES = 128
MESH = pl.DeviceIdType.MESH
ANY = pl.BlockSpec(memory_space=pl.ANY)
NEG = -1e30


def greet(peers):
    barrier = pltpu.get_barrier_semaphore()
    for peer in peers:
        pl.semaphore_signal(barrier, inc=1, device_id=peer, device_id_type=MESH)
    pl.semaphore_wait(barrier, len(peers))


def remote(src, dst, send, recv, peer):
    return pltpu.make_async_remote_copy(
        src_ref=src, dst_ref=dst, send_sem=send, recv_sem=recv, device_id=peer, device_id_type=MESH
    )


def group_of(mesh, width):
    for size in (4, 2):
        if mesh.shape["sp"] % size == 0 and width % (size * LANES) == 0:
            return size
    return 1


def gather_kernel(n_sp, group, hid_ref, wk_ref, wv_ref, hid_out, wk_out, wv_out, hs, hr, fs, fr, ws, wr, local):
    s = lax.axis_index("sp")
    t = lax.axis_index("tp")
    rows = hid_ref.shape[0]
    half_rows = rows // 2
    depth, width = wk_ref.shape
    part = width // group
    c = lax.rem(s, group)
    base = s - c
    half = lax.rem(t, 2)
    sibling = (s, t + 1 - 2 * half)
    near = [base + lax.rem(c + k, group) for k in range(1, group)]
    far = [lax.rem(s + k, n_sp) for k in range(1, n_sp)]
    greet([(peer, t) for peer in far] + [sibling])
    mine = pl.ds(pl.multiple_of(half * half_rows, half_rows), half_rows)

    copies = []
    for k, peer in enumerate(near):
        copies.append(remote(hid_ref.at[mine], hid_out.at[c, mine], hs.at[k], hr.at[k], (peer, t)))
        copies[-1].start()
    weights = []
    for k, peer in enumerate(far):
        cols = pl.ds(pl.multiple_of(lax.rem(peer, group) * part, LANES), part)
        into = pl.ds(pl.multiple_of(s * depth, depth), depth)
        for j, (src, dst) in enumerate(((wk_ref, wk_out), (wv_ref, wv_out))):
            weights.append(remote(src.at[:, cols], dst.at[into], ws.at[2 * k + j], wr.at[2 * k + j], (peer, t)))
            weights[-1].start()
    own = remote(hid_ref, hid_out.at[c], hs.at[group - 1], hr.at[group - 1], sibling)
    own.start()
    cols = pl.ds(pl.multiple_of(c * part, LANES), part)
    into = pl.ds(pl.multiple_of(s * depth, depth), depth)
    kept = [
        pltpu.make_async_copy(wk_ref.at[:, cols], wk_out.at[into], local.at[0]),
        pltpu.make_async_copy(wv_ref.at[:, cols], wv_out.at[into], local.at[1]),
    ]
    for copy in kept:
        copy.start()
    forwards = []
    for k in range(1, group):
        copies[k - 1].wait_recv()
        slot = hid_out.at[lax.rem(c + group - k, group), mine]
        forwards.append(remote(slot, slot, fs.at[k - 1], fr.at[k - 1], sibling))
        forwards[-1].start()
    for copy in copies:
        copy.wait_send()
    for copy in forwards + weights + [own] + kept:
        copy.wait()


def gather(mesh, group, hidden, key_proj, value_proj):
    n_sp = mesh.shape["sp"]
    depth, width = key_proj.shape
    part = width // group
    dma = pltpu.SemaphoreType.DMA
    weight = jax.ShapeDtypeStruct((n_sp * depth, part), key_proj.dtype)
    return pl.pallas_call(
        functools.partial(gather_kernel, n_sp, group),
        out_shape=(jax.ShapeDtypeStruct((group,) + hidden.shape, hidden.dtype), weight, weight),
        in_specs=[ANY] * 3,
        out_specs=(ANY,) * 3,
        scratch_shapes=[
            dma((group,)), dma((group,)), dma((group,)), dma((group,)),
            dma((2 * n_sp,)), dma((2 * n_sp,)), dma((2,)),
        ],
        compiler_params=pltpu.CompilerParams(collective_id=0, has_side_effects=True),
        name="gather_blocks",
    )(hidden, key_proj, value_proj)


def project_kernel(part, hid_ref, gain_ref, wq_ref, wk_ref, wv_ref, cos_ref, sin_ref, nat_ref, res_ref, scr):
    x = hid_ref[...].astype(jnp.float32)
    normed = x * lax.rsqrt(jnp.mean(x * x, axis=-1, keepdims=True) + EPS) * gain_ref[...]
    normed = normed.astype(jnp.bfloat16)
    rows = x.shape[0]
    front = lax.rem(lax.broadcasted_iota(jnp.int32, (rows, LANES), 1), HEAD_DIM) < HEAD_DIM // 2
    for j, w_ref in enumerate((wq_ref, wk_ref, wv_ref)):
        out = jnp.dot(normed, w_ref[...], preferred_element_type=jnp.float32)
        for i in range(part // LANES):
            u = out[:, i * LANES:(i + 1) * LANES]
            if j < 2:
                swapped = jnp.where(
                    front,
                    pltpu.roll(u, LANES - HEAD_DIM // 2, 1),
                    pltpu.roll(u, HEAD_DIM // 2, 1),
                )
                u = u * cos_ref[...] + swapped * sin_ref[...]
            if j == 0:
                u = u * HEAD_DIM ** (-0.5)
            scr[j * (part // LANES) + i] = u
    for i in range(3 * part // LANES):
        cols = pl.ds(i * LANES, LANES)
        nat_ref[:, cols] = scr[i].astype(jnp.bfloat16)
        for r in range(WIDE):
            res_ref[r, :, cols] = scr[i, pl.ds(r, rows // WIDE, stride=WIDE), :].astype(jnp.bfloat16)


def project(hid, gain, wq, wk, wv, cos_part, sin_part):
    rows, depth = hid.shape
    part = wk.shape[1]
    block = 256
    whole = pl.BlockSpec((depth, part), lambda i: (0, 0))
    table = pl.BlockSpec((block, LANES), lambda i: (i, 0))
    return pl.pallas_call(
        functools.partial(project_kernel, part),
        grid=(rows // block,),
        out_shape=(
            jax.ShapeDtypeStruct((rows, 3 * part), jnp.bfloat16),
            jax.ShapeDtypeStruct((WIDE, rows // WIDE, 3 * part), jnp.bfloat16),
        ),
        in_specs=[
            pl.BlockSpec((block, depth), lambda i: (i, 0)),
            pl.BlockSpec((1, depth), lambda i: (0, 0)),
            whole, whole, whole, table, table,
        ],
        out_specs=(
            pl.BlockSpec((block, 3 * part), lambda i: (i, 0)),
            pl.BlockSpec((WIDE, block // WIDE, 3 * part), lambda i: (0, i, 0)),
        ),
        scratch_shapes=[pltpu.VMEM((3 * part // LANES, block, LANES), jnp.float32)],
        compiler_params=pltpu.CompilerParams(vmem_limit_bytes=50 * 1024 * 1024),
        cost_estimate=pl.CostEstimate(flops=6 * rows * depth * part, bytes_accessed=2 * rows * depth, transcendentals=0),
        name="project_rows",
    )(hid, gain, wq, wk, wv, cos_part, sin_part)


def halo_kernel(n_sp, group, behind, part, nat_ref, res_ref, res_out, nat_out, send, recv):
    s = lax.axis_index("sp")
    t = lax.axis_index("tp")
    after = [lax.rem(s + b * group, n_sp) for b in range(1, behind + 1)]
    before = [lax.rem(s + n_sp - b * group, n_sp) for b in range(1, behind + 1)]
    greet([(peer, t) for peer in after + before])
    cols = pl.ds(part, 2 * part)
    last = pl.ds(nat_ref.shape[0] - SPAN, SPAN)
    copies = [remote(nat_ref.at[last, cols], nat_out, send.at[0], recv.at[0], (after[0], t))]
    for b in range(1, behind + 1):
        copies.append(
            remote(res_ref.at[:, :, cols], res_out.at[behind - b], send.at[b], recv.at[b], (after[b - 1], t))
        )
    for copy in copies:
        copy.start()
    for copy in copies:
        copy.wait()


def halo(mesh, group, behind, nat, res):
    part = nat.shape[1] // 3
    dma = pltpu.SemaphoreType.DMA
    return pl.pallas_call(
        functools.partial(halo_kernel, mesh.shape["sp"], group, behind, part),
        out_shape=(
            jax.ShapeDtypeStruct((behind, WIDE, res.shape[1], 2 * part), jnp.bfloat16),
            jax.ShapeDtypeStruct((SPAN, 2 * part), jnp.bfloat16),
        ),
        in_specs=[ANY] * 2,
        out_specs=(ANY,) * 2,
        scratch_shapes=[dma((behind + 1,)), dma((behind + 1,))],
        compiler_params=pltpu.CompilerParams(collective_id=1, has_side_effects=True),
        name="send_earlier",
    )(nat, res)


def attend_kernel(
    group, behind,
    qn, kn, vn, qr, kr, vr, hkr, hvr, hkn, hvn,
    out_ref, lw_ref,
    kx, vx, kw, vw, acc4, m4, l4, acc16, m16, l16, b1, b4, b16,
):
    rows = qn.shape[0]
    steps = rows // WIDE
    block = min(SPAN, steps)
    g = lax.axis_index("sp") // group
    f32 = jnp.float32
    for b in range(behind):
        kx[:, b * steps:(b + 1) * steps, :] = hkr[b]
        vx[:, b * steps:(b + 1) * steps, :] = hvr[b]
    kx[:, SPAN:, :] = kr[...]
    vx[:, SPAN:, :] = vr[...]
    kw[:SPAN, :] = hkn[...]
    vw[:SPAN, :] = hvn[...]
    kw[SPAN:, :] = kn[...]
    vw[SPAN:, :] = vn[...]

    def put_bias(ref, near, count, first_of):
        shape = ref.shape[1:]
        a = lax.broadcasted_iota(jnp.int32, shape, 0)
        b = lax.broadcasted_iota(jnp.int32, shape, 1)
        distance, place = near(a, b)
        band = (distance >= 0) & (distance <= SPAN)
        ref[0] = jnp.where(band & (place + first_of >= 0), 0.0, NEG).astype(f32)
        ref[1] = jnp.where(band, 0.0, NEG).astype(f32)

    def plain(a, b):
        return a + SPAN - b, b - SPAN

    def woven(a, b):
        return 4 * (a % 32 + 32 - b % 64) + a // 32 - b // 64, b % 64 - 32

    put_bias(b1, plain, 0, g * rows)
    put_bias(b16, plain, 0, g * steps)
    put_bias(b4, woven, 0, g * steps)

    def tile(q, k, v, bias):
        count = q.shape[0]
        low = lax.broadcasted_iota(jnp.int32, (count, LANES), 1) < HEAD_DIM
        low_q = low.astype(f32).astype(jnp.bfloat16)
        both = jnp.concatenate([q * low_q, q * (1 - low_q)], axis=0)
        s = lax.dot_general(both, k, (((1,), (1,)), ((), ())), preferred_element_type=f32)
        s = s + jnp.concatenate([bias, bias], axis=0)
        m = jnp.max(s, axis=-1, keepdims=True)
        p = jnp.exp(s - m).astype(jnp.bfloat16)
        o = jnp.dot(p, jnp.concatenate([v, jnp.ones_like(v)], axis=1), preferred_element_type=f32)
        wide_m = jnp.broadcast_to(m, (2 * count, LANES))
        return (
            jnp.where(low, o[:count, :LANES], o[count:, :LANES]),
            jnp.where(low, wide_m[:count], wide_m[count:]),
            jnp.where(low, o[:count, LANES:], o[count:, LANES:]),
        )

    blocks16 = steps // block

    def step16(idx, _):
        r = idx // blocks16
        i = idx % blocks16
        at = pl.multiple_of(i * block, block)
        keys = pl.ds(at, block + SPAN)
        got = tile(qr[r, pl.ds(at, block), :], kx[r, keys, :], vx[r, keys, :], b16[jnp.minimum(i, 1)])
        for ref, value in zip((acc16, m16, l16), got):
            ref[pl.ds(r + WIDE * at, block, stride=WIDE), :] = value
        return 0

    lax.fori_loop(0, WIDE * blocks16, step16, 0, unroll=2)
    blocks4 = steps // 32

    def step4(idx, _):
        r = idx // blocks4
        i = idx % blocks4
        at = pl.multiple_of(i * 32, 32)
        keys = pl.ds(pl.multiple_of(at + SPAN - 32, 32), 64)
        got = tile(
            jnp.concatenate([qr[r + 4 * j, pl.ds(at, 32), :] for j in range(4)], axis=0),
            jnp.concatenate([kx[r + 4 * j, keys, :] for j in range(4)], axis=0),
            jnp.concatenate([vx[r + 4 * j, keys, :] for j in range(4)], axis=0),
            b4[jnp.minimum(i, 1)],
        )
        for ref, value in zip((acc4, m4, l4), got):
            for j in range(4):
                ref[pl.ds(r + 4 * j + WIDE * at, 32, stride=WIDE), :] = value[j * 32:(j + 1) * 32]
        return 0

    lax.fori_loop(0, 4 * blocks4, step4, 0, unroll=2)

    def step1(i, _):
        at = pl.multiple_of(i * SPAN, SPAN)
        here = pl.ds(at, SPAN)
        keys = pl.ds(at, 2 * SPAN)
        acc, m, l = tile(qn[here, :], kw[keys, :], vw[keys, :], b1[jnp.minimum(i, 1)])
        top = jnp.maximum(m, jnp.maximum(m4[here, :], m16[here, :]))
        e1, e4, e16 = (jnp.exp(x - top) for x in (m, m4[here, :], m16[here, :]))
        total = l * e1 + l4[here, :] * e4 + l16[here, :] * e16
        mixed = acc * e1 + acc4[here, :] * e4 + acc16[here, :] * e16
        out_ref[here, :] = (mixed / total).astype(out_ref.dtype)
        turned = jnp.transpose(top + jnp.log(total))
        lw_ref[0, 0:1, here] = turned[0:1]
        lw_ref[0, 1:2, here] = turned[HEAD_DIM:HEAD_DIM + 1]
        return 0

    lax.fori_loop(0, rows // SPAN, step1, 0, unroll=2)


def attend(mesh, group, behind, nat, res, res_halo, nat_halo):
    rows, part3 = nat.shape
    part = part3 // 3
    pairs = part // LANES
    steps = rows // WIDE
    block = min(SPAN, steps)

    def nat_spec(count, off):
        return pl.BlockSpec((count, LANES), lambda p: (0, p + off))

    def res_spec(off):
        return pl.BlockSpec((WIDE, steps, LANES), lambda p: (0, 0, p + off))

    def halo_spec(off):
        return pl.BlockSpec((behind, WIDE, steps, LANES), lambda p: (0, 0, 0, p + off))

    f32 = jnp.float32
    state = pltpu.VMEM((rows, LANES), f32)
    return pl.pallas_call(
        functools.partial(attend_kernel, group, behind),
        grid=(pairs,),
        out_shape=(
            jax.ShapeDtypeStruct((rows, part), jnp.bfloat16),
            jax.ShapeDtypeStruct((pairs, 2, rows), f32),
        ),
        in_specs=[
            nat_spec(rows, 0), nat_spec(rows, pairs), nat_spec(rows, 2 * pairs),
            res_spec(0), res_spec(pairs), res_spec(2 * pairs),
            halo_spec(0), halo_spec(pairs),
            nat_spec(SPAN, 0), nat_spec(SPAN, pairs),
        ],
        out_specs=(
            pl.BlockSpec((rows, LANES), lambda p: (0, p)),
            pl.BlockSpec((1, 2, rows), lambda p: (p, 0, 0)),
        ),
        scratch_shapes=[
            pltpu.VMEM((WIDE, SPAN + steps, LANES), jnp.bfloat16),
            pltpu.VMEM((WIDE, SPAN + steps, LANES), jnp.bfloat16),
            pltpu.VMEM((SPAN + rows, LANES), jnp.bfloat16),
            pltpu.VMEM((SPAN + rows, LANES), jnp.bfloat16),
            state, state, state, state, state, state,
            pltpu.VMEM((2, SPAN, 2 * SPAN), f32),
            pltpu.VMEM((2, SPAN, 2 * SPAN), f32),
            pltpu.VMEM((2, block, block + SPAN), f32),
        ],
        compiler_params=pltpu.CompilerParams(vmem_limit_bytes=56 * 1024 * 1024),
        cost_estimate=pl.CostEstimate(flops=6 * rows * 512 * part, bytes_accessed=8 * rows * part, transcendentals=0),
        name="attend_windows",
    )(nat, nat, nat, res, res, res, res_halo, res_halo, nat_halo, nat_halo)


def return_kernel(group, rows, att_ref, lw_ref, att_out, lw_out, send, recv, local):
    s = lax.axis_index("sp")
    t = lax.axis_index("tp")
    part = att_ref.shape[1]
    c = lax.rem(s, group)
    base = s - c
    peers = [lax.rem(c + k, group) for k in range(1, group)]
    if group > 1:
        greet([(base + peer, t) for peer in peers])
    cols = pl.ds(pl.multiple_of(c * part, LANES), part)

    def pieces(peer):
        span = pl.ds(pl.multiple_of(peer * rows, rows), rows)
        return ((att_ref.at[span], att_out.at[:, cols]), (lw_ref.at[:, :, span], lw_out.at[c]))

    copies = []
    for k, peer in enumerate(peers):
        for j, (src, dst) in enumerate(pieces(peer)):
            copies.append(remote(src, dst, send.at[2 * k + j], recv.at[2 * k + j], (base + peer, t)))
    for j, (src, dst) in enumerate(pieces(c)):
        copies.append(pltpu.make_async_copy(src, dst, local.at[j]))
    for copy in copies:
        copy.start()
    for copy in copies:
        copy.wait()


def give_back(mesh, group, att, lw):
    rows = att.shape[0] // group
    part = att.shape[1]
    pairs = part // LANES
    dma = pltpu.SemaphoreType.DMA
    return pl.pallas_call(
        functools.partial(return_kernel, group, rows),
        out_shape=(
            jax.ShapeDtypeStruct((rows, part * group), att.dtype),
            jax.ShapeDtypeStruct((group, pairs, 2, rows), lw.dtype),
        ),
        in_specs=[ANY] * 2,
        out_specs=(ANY,) * 2,
        scratch_shapes=[dma((2 * group,)), dma((2 * group,)), dma((2,))],
        compiler_params=pltpu.CompilerParams(
            collective_id=2 if group > 1 else None, has_side_effects=True
        ),
        name="give_back",
    )(att, lw)


def swap_kernel(n_tp, part_ref, out_ref, send, recv):
    s = lax.axis_index("sp")
    t = lax.axis_index("tp")
    peers = [lax.rem(t + k, n_tp) for k in range(1, n_tp)]
    greet([(s, peer) for peer in peers])
    copies = [
        remote(part_ref.at[peer], out_ref.at[k], send.at[k], recv.at[k], (s, peer))
        for k, peer in enumerate(peers)
    ]
    for copy in copies:
        copy.start()
    for copy in copies:
        copy.wait()


def swap(mesh, partial):
    n_tp = mesh.shape["tp"]
    dma = pltpu.SemaphoreType.DMA
    return pl.pallas_call(
        functools.partial(swap_kernel, n_tp),
        out_shape=jax.ShapeDtypeStruct((n_tp - 1,) + partial.shape[1:], partial.dtype),
        in_specs=[ANY],
        out_specs=ANY,
        scratch_shapes=[dma((n_tp,)), dma((n_tp,))],
        compiler_params=pltpu.CompilerParams(collective_id=3, has_side_effects=True),
        name="swap_partials",
    )(partial)


def tables(rows, offset):
    half = HEAD_DIM // 2
    frequency = ROPE_BASE ** (-(jnp.arange(half, dtype=jnp.float32) * 2.0 / HEAD_DIM))
    positions = (offset + jnp.arange(rows, dtype=jnp.int32)).astype(jnp.float32)
    angles = positions[:, None] * frequency[None, :]
    cos_part = jnp.cos(angles)
    sin_part = jnp.sin(angles)
    return (
        jnp.concatenate([cos_part] * 4, axis=1),
        jnp.concatenate([-sin_part, sin_part] * 2, axis=1),
    )


def body(mesh, hidden_in, pre_gain, query_proj, key_proj, value_proj, out_proj, post_gain):
    rows, depth = hidden_in.shape
    width = query_proj.shape[1]
    n_tp = mesh.shape["tp"]
    group = group_of(mesh, width)
    part = width // group
    s = lax.axis_index("sp")
    t = lax.axis_index("tp")
    c = lax.rem(s, group)
    all_rows = rows * group
    behind = -(-(WIDE * SPAN) // all_rows)
    hid, wk, wv = gather(mesh, group, hidden_in, key_proj, value_proj)
    wq = lax.dynamic_slice_in_dim(query_proj, c * part, part, axis=1)
    cos_part, sin_part = tables(all_rows, (s - c) * rows)
    nat, res = project(
        hid.reshape(all_rows, depth), pre_gain[None, :], wq, wk, wv, cos_part, sin_part
    )
    res_halo, nat_halo = halo(mesh, group, behind, nat, res)
    att, lw = attend(mesh, group, behind, nat, res, res_halo, nat_halo)
    attended, log_weight = give_back(mesh, group, att, lw)
    partial = jnp.dot(attended, out_proj, preferred_element_type=jnp.float32).astype(jnp.bfloat16)
    partial = partial.reshape(n_tp, rows // n_tp, depth)
    others = swap(mesh, partial)
    own = lax.dynamic_index_in_dim(partial, t, 0, keepdims=False)
    summed = own.astype(jnp.float32) + jnp.sum(others.astype(jnp.float32), axis=0)
    scale = lax.rsqrt(jnp.mean(summed * summed, axis=-1, keepdims=True) + EPS)
    layer_out = (summed * scale * post_gain).astype(jnp.bfloat16)
    return (layer_out, log_weight.reshape(width // HEAD_DIM, rows))


def solution(mesh):
    placed = (P("sp", None), P(), P(None, "tp"), P("sp", "tp"), P("sp", "tp"), P("tp", None), P())
    return jax.shard_map(
        functools.partial(body, mesh),
        mesh=mesh,
        in_specs=placed,
        out_specs=(P(("sp", "tp"), None), P("tp", "sp")),
        check_vma=False,
    )
```

time: 579 us -> 222 us (0.38); the launches traced: 570 us -> 221 us
  waiting for transfers between devices: 288 us -> 0 us
  Pallas kernels: 0 us -> 199 us
  local copies, waits for them, and re-layouts: 137 us -> 5.15 us
  matrix products: 76.2 us -> 6.18 us
  other arithmetic: 37.1 us -> 9.98 us
  starting transfers between devices: 16.2 us -> 0 us
  between operations: 14.8 us -> 0.75 us
    pallas_call x0 -> x6, Pallas kernels: none -> 199 us  [the longest x1 83.1 us: gather(): pl.pallas_call(functools.partial(gather_kernel, n_sp, group), out_shape=(...]
    all_gather x2 -> x0, waiting for transfers between devices: 142 us -> none  [the longest x1 72.6 us: body(): lax.all_gather(key_proj, 'sp', axis=0, tiled=True)]
    reduce_scatter x1 -> x0, waiting for transfers between devices: 89.2 us -> none  [body(): lax.psum_scatter(jnp.dot(attended, out_proj, preferred_element_type=jnp.f...]
    dot_general x9 -> x0, matrix products: 72.5 us -> none  [the longest x3 29.6 us: window_group(): jnp.einsum('bqrhe,bkrhe->brhqk', query_blocks, key_sets, preferred_elemen...]
    ppermute x4 -> x0, waiting for transfers between devices: 55.7 us -> none  [passed_along(): lax.ppermute(value, axis, [(source, source + steps) for source in range(f...]
    another operation x11 -> x0, local copies, waits for them, and re-layouts: 54.7 us -> none
    concatenate x7 -> x0, local copies, waits for them, and re-layouts: 29.5 us -> none  [the longest x6 15.7 us: rotate(): jnp.concatenate([front_half * cos_part - back_half * sin_part, back_half...]
    reduce_sum x6 -> x1, other arithmetic: 27.5 us -> 1.74 us  [body(): scale = lax.rsqrt(jnp.mean(summed * summed, axis=-1, keepdims=True) + EPS)]
  transfers between devices with their start and end apart: 7 -> 0, of which waited for: 6 -> 0; matrix products, arithmetic and copies ran while one was open for 8% -> 0% of each run, Pallas kernels for 0% -> 0%
where the time goes in v1:
time: 222 us; the launch traced here: 221 us
  Pallas kernels  199 us (90%)
  other arithmetic  9.98 us (4%)
  matrix products  6.18 us (3%)
  local copies, waits for them, and re-layouts  5.15 us (2%)
    pallas_call x1, Pallas kernels, gather(): pl.pallas_call(functools.partial(gather_kernel, n_sp, group), out_shape=(...  83.1 us
    pallas_call x1, Pallas kernels, halo(): pl.pallas_call(functools.partial(halo_kernel, mesh.shape['sp'], group, be...  52.5 us
    pallas_call x1, Pallas kernels, attend(): pl.pallas_call(functools.partial(attend_kernel, group, behind), grid=(pai...  30.6 us
    pallas_call x1, Pallas kernels, give_back(): pl.pallas_call(functools.partial(return_kernel, group, rows), out_shape=(...  15.2 us
    pallas_call x1, Pallas kernels, project(): pl.pallas_call(functools.partial(project_kernel, part), grid=(rows // blo...  14.6 us
    dot_general x1, matrix products, body(): jnp.dot(attended, out_proj, preferred_element_type=jnp.float32)  6.18 us

profile of v1, /device:TPU:0, one launch (start us, length us, event | category | flops | bytes accessed | tf_op | source)
XLA Modules:
  0.0 221.1 jit_solution(1922671531789440705)
XLA Ops:
  0.7 1.3 constant_dynamic-slice_fusion.wq_ref
  2.0 3.7 %fusion.3 = (f32[2048,32]{1,0:T(8,128)S(1)}, f32[2048,32]{1,0:T(8,128)S(1)}, f32[2048,32]{1,0:T(8,128)S(1)}) fusion(f32[32]{0:T(128)S(1)} %negate_power_fusion, f32[2048]{0:T(1024)S(1)} %add_convert_fusion), kind=kLoop, calls=%fused_computation.11 | loop fusion | flops 131072 | bytes 794752 | tf_op jit(solution)/shard_map/neg | solution.py:447
  5.7 3.0 %pad_maximum_fusion = (f32[2048,128]{1,0:T(8,128)}, f32[2048,128]{1,0:T(8,128)}) fusion(f32[2048,32]{1,0:T(8,128)S(1)} %get-tuple-element.26, f32[2048,32]{1,0:T(8,128)S(1)} %get-tuple-element.25, f32[2048,32]{1,0:T(8,128)S(1)} %get-tuple-element.24), kind=kLoop, calls=%fused_computation.9 | loop fusion | flops 1572864 | bytes 2883584 | tf_op jit(solution)/shard_map/concatenate | solution.py:446
  8.7 0.0 copy-start.2
  8.7 83.1 %gather_blocks.1 = (bf16[4,512,2048]{2,1,0:T(8,128)(2,1)}, bf16[2048,256]{1,0:T(8,128)(2,1)}, bf16[2048,256]{1,0:T(8,128)(2,1)}) custom-call(bf16[512,2048]{1,0:T(8,128)(2,1)} %hid_ref.1, bf16[128,1024]{1,0:T(8,128)(2,1)} %wk_ref.1, bf16[128,1024]{1,0:T(8,128)(2,1)} %wv_ref.1), custom_call_target="tpu_custom_call" | custom-call | tf_op jit(solution)/shard_map/gather_blocks/pallas_call | solution.py:96
  91.8 0.0 copy-done.2
  91.9 0.0 copy-start
  91.9 1.2 copy-done
  93.1 0.0 copy-start.1
  93.1 1.2 copy-done.1
  94.3 14.6 %project_rows.1 = (bf16[2048,768]{1,0:T(8,128)(2,1)}, bf16[16,128,768]{2,1,0:T(8,128)(2,1)}) custom-call(bf16[2048,2048]{1,0:T(8,128)(2,1)} %bitcast.18, f32[1,2048]{1,0:T(1,128)S(1)} %bitcast.14, bf16[2048,256]{1,0:T(8,128)(2,1)S(1)} %constant_dynamic-slice_fusion.wq_ref, bf16[2048,256]{1,0:T(8,128)(2,1)S(1)} %copy-done, bf16[2048,256]{1,0:T(8,128)(2,1)S(1)} %copy-done.1, ...), custom_call_target="tpu_custom_call" | custom-call | flops 6442450944 | bytes 8388608 | tf_op jit(solution)/shard_map/project_rows/pallas_call | solution.py:143
  108.9 52.5 %send_earlier.1 = (bf16[1,16,128,512]{3,2,1,0:T(8,128)(2,1)}, bf16[128,512]{1,0:T(8,128)(2,1)}) custom-call(bf16[2048,768]{1,0:T(8,128)(2,1)} %get-tuple-element.16.nat_ref.qn.kn.vn, bf16[16,128,768]{2,1,0:T(8,128)(2,1)} %get-tuple-element.17.res_ref.qr.kr.vr), custom_call_target="tpu_custom_call" | custom-call | tf_op jit(solution)/shard_map/send_earlier/pallas_call | solution.py:188
  161.4 30.6 %attend_windows.1 = (bf16[2048,256]{1,0:T(8,128)(2,1)}, f32[2,2,2048]{2,1,0:T(2,128)}) custom-call(bf16[2048,768]{1,0:T(8,128)(2,1)} %get-tuple-element.16.nat_ref.qn.kn.vn, bf16[2048,768]{1,0:T(8,128)(2,1)} %get-tuple-element.16.nat_ref.qn.kn.vn, bf16[2048,768]{1,0:T(8,128)(2,1)} %get-tuple-element.16.nat_ref.qn.kn.vn, ...), custom_call_target="tpu_custom_call" | custom-call | flops 1610612736 | bytes 4194304 | tf_op jit(solution)/shard_map/attend_windows/pallas_call | solution.py:328
  192.0 15.2 %give_back.1 = (bf16[512,1024]{1,0:T(8,128)(2,1)}, f32[4,2,2,512]{3,2,1,0:T(2,128)}) custom-call(bf16[2048,256]{1,0:T(8,128)(2,1)} %get-tuple-element.20.att_ref, f32[2,2,2048]{2,1,0:T(2,128)} %get-tuple-element.21.lw_ref), custom_call_target="tpu_custom_call" | custom-call | tf_op jit(solution)/shard_map/give_back/pallas_call | solution.py:393
  207.2 1.4 reshape.38
  208.6 6.2 %convolution_convert_fusion = bf16[512,2048]{1,0:T(8,128)(2,1)} fusion(bf16[512,1024]{1,0:T(8,128)(2,1)} %get-tuple-element.22, bf16[1024,2048]{1,0:T(8,128)(2,1)} %param.12), kind=kOutput, calls=%fused_computation | convolution fusion | flops 2148532224 | bytes 7340032 | tf_op jit(solution)/shard_map/dot_general | solution.py:471
  214.8 0.0 copy-start.4
  214.8 0.0 copy-start.5
  214.8 3.0 %swap_partials.1 = bf16[1,256,2048]{2,1,0:T(8,128)(2,1)} custom-call(bf16[2,256,2048]{2,1,0:T(8,128)(2,1)} %bitcast.15), custom_call_target="tpu_custom_call" | custom-call | tf_op jit(solution)/shard_map/swap_partials/pallas_call | solution.py:427
  217.8 0.0 copy-done.4
  217.8 0.0 copy-start.3
  217.9 1.7 fusion
  219.6 0.0 copy-done.5
  219.6 0.0 copy-done.3
  219.6 1.5 fusion.2
  (3 shorter events, 0.0 us)
Async XLA Ops:
  8.7 83.1 %copy-start.2 = (f32[2048]{0:T(1024)S(1)}, f32[2048]{0:T(1024)}, u32[]{:S(2)}) copy-start(f32[2048]{0:T(1024)} %param.8) | copy-start | bytes 24580
  91.9 1.2 copy-start
  93.1 1.2 copy-start.1
  214.8 3.1 %copy-start.4 = (bf16[512,2048]{1,0:T(8,128)(2,1)S(1)}, bf16[512,2048]{1,0:T(8,128)(2,1)}, u32[]{:S(2)}) copy-start(bf16[512,2048]{1,0:T(8,128)(2,1)} %convolution_convert_fusion) | copy-start | bytes 6291460
  214.8 4.8 %copy-start.5 = (f32[2048]{0:T(1024)S(1)}, f32[2048]{0:T(1024)}, u32[]{:S(2)}) copy-start(f32[2048]{0:T(1024)} %param.13) | copy-start | bytes 24580
  217.8 1.8 copy-start.3

commit v2 on v1

--- a/solution.py
+++ b/solution.py
@@ -50,31 +50,40 @@
     half = lax.rem(t, 2)
     sibling = (s, t + 1 - 2 * half)
     near = [base + lax.rem(c + k, group) for k in range(1, group)]
-    far = [lax.rem(s + k, n_sp) for k in range(1, n_sp)]
-    greet([(peer, t) for peer in far] + [sibling])
+    far = [lax.rem(s + k * group, n_sp) for k in range(1, n_sp // group)]
+    greet([(peer, t) for peer in near + far] + [sibling])
     mine = pl.ds(pl.multiple_of(half * half_rows, half_rows), half_rows)
 
+    pairs = ((wk_ref, wk_out), (wv_ref, wv_out))
+    into = pl.ds(pl.multiple_of(s * depth, depth), depth)
+    cols = pl.ds(pl.multiple_of(c * part, LANES), part)
+    kept = [
+        pltpu.make_async_copy(src.at[:, cols], dst.at[into], local.at[j])
+        for j, (src, dst) in enumerate(pairs)
+    ]
+    for copy in kept:
+        copy.start()
+    weights = []
+    for k, peer in enumerate(near):
+        cols = pl.ds(pl.multiple_of((peer - base) * part, LANES), part)
+        for j, (src, dst) in enumerate(pairs):
+            weights.append(remote(src.at[:, cols], dst.at[into], ws.at[2 * k + j], wr.at[2 * k + j], (peer, t)))
+            weights[-1].start()
     copies = []
     for k, peer in enumerate(near):
         copies.append(remote(hid_ref.at[mine], hid_out.at[c, mine], hs.at[k], hr.at[k], (peer, t)))
         copies[-1].start()
-    weights = []
-    for k, peer in enumerate(far):
-        cols = pl.ds(pl.multiple_of(lax.rem(peer, group) * part, LANES), part)
-        into = pl.ds(pl.multiple_of(s * depth, depth), depth)
-        for j, (src, dst) in enumerate(((wk_ref, wk_out), (wv_ref, wv_out))):
-            weights.append(remote(src.at[:, cols], dst.at[into], ws.at[2 * k + j], wr.at[2 * k + j], (peer, t)))
-            weights[-1].start()
     own = remote(hid_ref, hid_out.at[c], hs.at[group - 1], hr.at[group - 1], sibling)
     own.start()
-    cols = pl.ds(pl.multiple_of(c * part, LANES), part)
-    into = pl.ds(pl.multiple_of(s * depth, depth), depth)
-    kept = [
-        pltpu.make_async_copy(wk_ref.at[:, cols], wk_out.at[into], local.at[0]),
-        pltpu.make_async_copy(wv_ref.at[:, cols], wv_out.at[into], local.at[1]),
-    ]
-    for copy in kept:
-        copy.start()
+    for copy in kept + weights:
+        copy.wait()
+    slot = pl.ds(pl.multiple_of(base * depth, depth), group * depth)
+    passed = []
+    for k, peer in enumerate(far):
+        for j, (_, dst) in enumerate(pairs):
+            at = 2 * (group - 1 + k) + j
+            passed.append(remote(dst.at[slot], dst.at[slot], ws.at[at], wr.at[at], (peer, t)))
+            passed[-1].start()
     forwards = []
     for k in range(1, group):
         copies[k - 1].wait_recv()
@@ -83,7 +92,7 @@
         forwards[-1].start()
     for copy in copies:
         copy.wait_send()
-    for copy in forwards + weights + [own] + kept:
+    for copy in forwards + passed + [own]:
         copy.wait()
 
 

time: 222 us -> 201 us (0.905)
  Pallas kernels: 199 us -> 178 us
    pallas_call x1, Pallas kernels: 83.1 us -> 62.8 us  [gather(): pl.pallas_call(functools.partial(gather_kernel, n_sp, group), out_shape=(...]
where the time goes in v2:
time: 201 us; the launch traced here: 200 us
  Pallas kernels  178 us (89%)
  other arithmetic  9.98 us (5%)
  matrix products  6.18 us (3%)
  local copies, waits for them, and re-layouts  5.15 us (3%)
    pallas_call x1, Pallas kernels, gather(): pl.pallas_call(functools.partial(gather_kernel, n_sp, group), out_shape=(...  62.8 us
    pallas_call x1, Pallas kernels, halo(): pl.pallas_call(functools.partial(halo_kernel, mesh.shape['sp'], group, be...  52.9 us
    pallas_call x1, Pallas kernels, attend(): pl.pallas_call(functools.partial(attend_kernel, group, behind), grid=(pai...  30.6 us
    pallas_call x1, Pallas kernels, project(): pl.pallas_call(functools.partial(project_kernel, part), grid=(rows // blo...  14.6 us
    pallas_call x1, Pallas kernels, give_back(): pl.pallas_call(functools.partial(return_kernel, group, rows), out_shape=(...  14.2 us
    dot_general x1, matrix products, body(): jnp.dot(attended, out_proj, preferred_element_type=jnp.float32)  6.18 us

profile of v2, /device:TPU:0, one launch (start us, length us, event | category | flops | bytes accessed | tf_op | source)
XLA Modules:
  0.0 200.2 jit_solution(15147087462241170038)
XLA Ops:
  0.7 1.3 constant_dynamic-slice_fusion.wq_ref
  2.0 3.7 %fusion.3 = (f32[2048,32]{1,0:T(8,128)S(1)}, f32[2048,32]{1,0:T(8,128)S(1)}, f32[2048,32]{1,0:T(8,128)S(1)}) fusion(f32[32]{0:T(128)S(1)} %negate_power_fusion, f32[2048]{0:T(1024)S(1)} %add_convert_fusion), kind=kLoop, calls=%fused_computation.11 | loop fusion | flops 131072 | bytes 794752 | tf_op jit(solution)/shard_map/neg | solution.py:456
  5.7 3.0 %pad_maximum_fusion = (f32[2048,128]{1,0:T(8,128)}, f32[2048,128]{1,0:T(8,128)}) fusion(f32[2048,32]{1,0:T(8,128)S(1)} %get-tuple-element.26, f32[2048,32]{1,0:T(8,128)S(1)} %get-tuple-element.25, f32[2048,32]{1,0:T(8,128)S(1)} %get-tuple-element.24), kind=kLoop, calls=%fused_computation.9 | loop fusion | flops 1572864 | bytes 2883584 | tf_op jit(solution)/shard_map/concatenate | solution.py:455
  8.7 0.0 copy-start.2
  8.7 62.8 %gather_blocks.1 = (bf16[4,512,2048]{2,1,0:T(8,128)(2,1)}, bf16[2048,256]{1,0:T(8,128)(2,1)}, bf16[2048,256]{1,0:T(8,128)(2,1)}) custom-call(bf16[512,2048]{1,0:T(8,128)(2,1)} %hid_ref.1, bf16[128,1024]{1,0:T(8,128)(2,1)} %wk_ref.1, bf16[128,1024]{1,0:T(8,128)(2,1)} %wv_ref.1), custom_call_target="tpu_custom_call" | custom-call | tf_op jit(solution)/shard_map/gather_blocks/pallas_call | solution.py:105
  71.5 0.0 copy-done.2
  71.5 0.0 copy-start
  71.5 1.2 copy-done
  72.7 0.0 copy-start.1
  72.7 1.2 copy-done.1
  73.9 14.6 %project_rows.1 = (bf16[2048,768]{1,0:T(8,128)(2,1)}, bf16[16,128,768]{2,1,0:T(8,128)(2,1)}) custom-call(bf16[2048,2048]{1,0:T(8,128)(2,1)} %bitcast.18, f32[1,2048]{1,0:T(1,128)S(1)} %bitcast.14, bf16[2048,256]{1,0:T(8,128)(2,1)S(1)} %constant_dynamic-slice_fusion.wq_ref, bf16[2048,256]{1,0:T(8,128)(2,1)S(1)} %copy-done, bf16[2048,256]{1,0:T(8,128)(2,1)S(1)} %copy-done.1, ...), custom_call_target="tpu_custom_call" | custom-call | flops 6442450944 | bytes 8388608 | tf_op jit(solution)/shard_map/project_rows/pallas_call | solution.py:152
  88.6 52.9 %send_earlier.1 = (bf16[1,16,128,512]{3,2,1,0:T(8,128)(2,1)}, bf16[128,512]{1,0:T(8,128)(2,1)}) custom-call(bf16[2048,768]{1,0:T(8,128)(2,1)} %get-tuple-element.16.nat_ref.qn.kn.vn, bf16[16,128,768]{2,1,0:T(8,128)(2,1)} %get-tuple-element.17.res_ref.qr.kr.vr), custom_call_target="tpu_custom_call" | custom-call | tf_op jit(solution)/shard_map/send_earlier/pallas_call | solution.py:197
  141.5 30.6 %attend_windows.1 = (bf16[2048,256]{1,0:T(8,128)(2,1)}, f32[2,2,2048]{2,1,0:T(2,128)}) custom-call(bf16[2048,768]{1,0:T(8,128)(2,1)} %get-tuple-element.16.nat_ref.qn.kn.vn, bf16[2048,768]{1,0:T(8,128)(2,1)} %get-tuple-element.16.nat_ref.qn.kn.vn, bf16[2048,768]{1,0:T(8,128)(2,1)} %get-tuple-element.16.nat_ref.qn.kn.vn, ...), custom_call_target="tpu_custom_call" | custom-call | flops 1610612736 | bytes 4194304 | tf_op jit(solution)/shard_map/attend_windows/pallas_call | solution.py:337
  172.0 14.2 %give_back.1 = (bf16[512,1024]{1,0:T(8,128)(2,1)}, f32[4,2,2,512]{3,2,1,0:T(2,128)}) custom-call(bf16[2048,256]{1,0:T(8,128)(2,1)} %get-tuple-element.20.att_ref, f32[2,2,2048]{2,1,0:T(2,128)} %get-tuple-element.21.lw_ref), custom_call_target="tpu_custom_call" | custom-call | tf_op jit(solution)/shard_map/give_back/pallas_call | solution.py:402
  186.3 1.4 reshape.38
  187.7 6.2 %convolution_convert_fusion = bf16[512,2048]{1,0:T(8,128)(2,1)} fusion(bf16[512,1024]{1,0:T(8,128)(2,1)} %get-tuple-element.22, bf16[1024,2048]{1,0:T(8,128)(2,1)} %param.12), kind=kOutput, calls=%fused_computation | convolution fusion | flops 2148532224 | bytes 7340032 | tf_op jit(solution)/shard_map/dot_general | solution.py:480
  193.9 0.0 copy-start.4
  193.9 0.0 copy-start.5
  193.9 3.0 %swap_partials.1 = bf16[1,256,2048]{2,1,0:T(8,128)(2,1)} custom-call(bf16[2,256,2048]{2,1,0:T(8,128)(2,1)} %bitcast.15), custom_call_target="tpu_custom_call" | custom-call | tf_op jit(solution)/shard_map/swap_partials/pallas_call | solution.py:436
  196.9 0.0 copy-done.4
  196.9 0.0 copy-start.3
  196.9 1.7 fusion
  198.7 0.0 copy-done.5
  198.7 0.0 copy-done.3
  198.7 1.5 fusion.2
  (3 shorter events, 0.0 us)
Async XLA Ops:
  8.7 62.8 %copy-start.2 = (f32[2048]{0:T(1024)S(1)}, f32[2048]{0:T(1024)}, u32[]{:S(2)}) copy-start(f32[2048]{0:T(1024)} %param.8) | copy-start | bytes 24580
  71.5 1.2 copy-start
  72.7 1.2 copy-start.1
  193.9 3.1 %copy-start.4 = (bf16[512,2048]{1,0:T(8,128)(2,1)S(1)}, bf16[512,2048]{1,0:T(8,128)(2,1)}, u32[]{:S(2)}) copy-start(bf16[512,2048]{1,0:T(8,128)(2,1)} %convolution_convert_fusion) | copy-start | bytes 6291460
  193.9 4.8 %copy-start.5 = (f32[2048]{0:T(1024)S(1)}, f32[2048]{0:T(1024)}, u32[]{:S(2)}) copy-start(f32[2048]{0:T(1024)} %param.13) | copy-start | bytes 24580
  196.9 1.8 copy-start.3

commit v3 on v2

--- a/solution.py
+++ b/solution.py
@@ -172,60 +172,59 @@
     )(hid, gain, wq, wk, wv, cos_part, sin_part)
 
 
-def halo_kernel(n_sp, group, behind, part, nat_ref, res_ref, res_out, nat_out, send, recv):
-    s = lax.axis_index("sp")
-    t = lax.axis_index("tp")
-    after = [lax.rem(s + b * group, n_sp) for b in range(1, behind + 1)]
-    before = [lax.rem(s + n_sp - b * group, n_sp) for b in range(1, behind + 1)]
-    greet([(peer, t) for peer in after + before])
-    cols = pl.ds(part, 2 * part)
-    last = pl.ds(nat_ref.shape[0] - SPAN, SPAN)
-    copies = [remote(nat_ref.at[last, cols], nat_out, send.at[0], recv.at[0], (after[0], t))]
-    for b in range(1, behind + 1):
-        copies.append(
-            remote(res_ref.at[:, :, cols], res_out.at[behind - b], send.at[b], recv.at[b], (after[b - 1], t))
-        )
-    for copy in copies:
-        copy.start()
-    for copy in copies:
-        copy.wait()
-
-
-def halo(mesh, group, behind, nat, res):
-    part = nat.shape[1] // 3
-    dma = pltpu.SemaphoreType.DMA
-    return pl.pallas_call(
-        functools.partial(halo_kernel, mesh.shape["sp"], group, behind, part),
-        out_shape=(
-            jax.ShapeDtypeStruct((behind, WIDE, res.shape[1], 2 * part), jnp.bfloat16),
-            jax.ShapeDtypeStruct((SPAN, 2 * part), jnp.bfloat16),
-        ),
-        in_specs=[ANY] * 2,
-        out_specs=(ANY,) * 2,
-        scratch_shapes=[dma((behind + 1,)), dma((behind + 1,))],
-        compiler_params=pltpu.CompilerParams(collective_id=1, has_side_effects=True),
-        name="send_earlier",
-    )(nat, res)
-
-
 def attend_kernel(
-    group, behind,
-    qn, kn, vn, qr, kr, vr, hkr, hvr, hkn, hvn,
+    n_sp, group, behind, pairs,
+    nat_ref, res_ref, qn, kn, vn, qr, kr, vr,
     out_ref, lw_ref,
-    kx, vx, kw, vw, acc4, m4, l4, acc16, m16, l16, b1, b4, b16,
+    kx_all, vx_all, kw_all, vw_all, acc1, m1, l1, acc4, m4, l4, acc16, m16, l16, b1, b4, b16, send, recv,
 ):
     rows = qn.shape[0]
     steps = rows // WIDE
     block = min(SPAN, steps)
     g = lax.axis_index("sp") // group
     f32 = jnp.float32
-    for b in range(behind):
-        kx[:, b * steps:(b + 1) * steps, :] = hkr[b]
-        vx[:, b * steps:(b + 1) * steps, :] = hvr[b]
+    s = lax.axis_index("sp")
+    t = lax.axis_index("tp")
+    p = pl.program_id(0)
+    after = [lax.rem(s + b * group, n_sp) for b in range(1, behind + 1)]
+    before = [lax.rem(s + n_sp - b * group, n_sp) for b in range(1, behind + 1)]
+    last = pl.ds(rows - SPAN, SPAN)
+
+    def early(pair):
+        copies = []
+        for j, (ref, first) in enumerate(((kw_all, pairs), (vw_all, 2 * pairs))):
+            cols = pl.ds(pl.multiple_of((first + pair) * LANES, LANES), LANES)
+            copies.append(remote(
+                nat_ref.at[last, cols], ref.at[pair, pl.ds(0, SPAN)], send.at[pair, j], recv.at[pair, j], (after[0], t)
+            ))
+        return copies
+
+    def late(pair):
+        copies = []
+        for j, (ref, first) in enumerate(((kx_all, pairs), (vx_all, 2 * pairs))):
+            cols = pl.ds(pl.multiple_of((first + pair) * LANES, LANES), LANES)
+            for b in range(1, behind + 1):
+                at = 2 * b + j
+                copies.append(remote(
+                    res_ref.at[:, :, cols],
+                    ref.at[pair, :, pl.ds((behind - b) * steps, steps)],
+                    send.at[pair, at], recv.at[pair, at], (after[b - 1], t),
+                ))
+        return copies
+
+    @pl.when(p == 0)
+    def _():
+        greet([(peer, t) for peer in after + before])
+        for pair in range(pairs):
+            for copy in early(pair):
+                copy.start()
+        for pair in range(pairs):
+            for copy in late(pair):
+                copy.start()
+
+    kx, vx, kw, vw = (ref.at[p] for ref in (kx_all, vx_all, kw_all, vw_all))
     kx[:, SPAN:, :] = kr[...]
     vx[:, SPAN:, :] = vr[...]
-    kw[:SPAN, :] = hkn[...]
-    vw[:SPAN, :] = hvn[...]
     kw[SPAN:, :] = kn[...]
     vw[SPAN:, :] = vn[...]
 
@@ -277,46 +276,61 @@
             ref[pl.ds(r + WIDE * at, block, stride=WIDE), :] = value
         return 0
 
-    lax.fori_loop(0, WIDE * blocks16, step16, 0, unroll=2)
     blocks4 = steps // 32
 
-    def step4(idx, _):
-        r = idx // blocks4
-        i = idx % blocks4
-        at = pl.multiple_of(i * 32, 32)
-        keys = pl.ds(pl.multiple_of(at + SPAN - 32, 32), 64)
+    def step4(r, i):
+        at = pl.multiple_of(i * 32, 32) if not isinstance(i, int) else i * 32
+        keys = pl.ds(pl.multiple_of(at + SPAN - 32, 32) if not isinstance(i, int) else at + SPAN - 32, 64)
         got = tile(
             jnp.concatenate([qr[r + 4 * j, pl.ds(at, 32), :] for j in range(4)], axis=0),
             jnp.concatenate([kx[r + 4 * j, keys, :] for j in range(4)], axis=0),
             jnp.concatenate([vx[r + 4 * j, keys, :] for j in range(4)], axis=0),
-            b4[jnp.minimum(i, 1)],
+            b4[0 if isinstance(i, int) else 1],
         )
         for ref, value in zip((acc4, m4, l4), got):
             for j in range(4):
                 ref[pl.ds(r + 4 * j + WIDE * at, 32, stride=WIDE), :] = value[j * 32:(j + 1) * 32]
         return 0
 
-    lax.fori_loop(0, 4 * blocks4, step4, 0, unroll=2)
 
     def step1(i, _):
         at = pl.multiple_of(i * SPAN, SPAN)
         here = pl.ds(at, SPAN)
         keys = pl.ds(at, 2 * SPAN)
-        acc, m, l = tile(qn[here, :], kw[keys, :], vw[keys, :], b1[jnp.minimum(i, 1)])
-        top = jnp.maximum(m, jnp.maximum(m4[here, :], m16[here, :]))
-        e1, e4, e16 = (jnp.exp(x - top) for x in (m, m4[here, :], m16[here, :]))
-        total = l * e1 + l4[here, :] * e4 + l16[here, :] * e16
-        mixed = acc * e1 + acc4[here, :] * e4 + acc16[here, :] * e16
+        got = tile(qn[here, :], kw[keys, :], vw[keys, :], b1[jnp.minimum(i, 1)])
+        for ref, value in zip((acc1, m1, l1), got):
+            ref[here, :] = value
+        return 0
+
+    def merge(i, _):
+        here = pl.ds(pl.multiple_of(i * SPAN, SPAN), SPAN)
+        tops = (m1[here, :], m4[here, :], m16[here, :])
+        top = jnp.maximum(tops[0], jnp.maximum(tops[1], tops[2]))
+        e1, e4, e16 = (jnp.exp(x - top) for x in tops)
+        total = l1[here, :] * e1 + l4[here, :] * e4 + l16[here, :] * e16
+        mixed = acc1[here, :] * e1 + acc4[here, :] * e4 + acc16[here, :] * e16
         out_ref[here, :] = (mixed / total).astype(out_ref.dtype)
         turned = jnp.transpose(top + jnp.log(total))
         lw_ref[0, 0:1, here] = turned[0:1]
         lw_ref[0, 1:2, here] = turned[HEAD_DIM:HEAD_DIM + 1]
         return 0
 
+    if blocks4 > 1:
+        lax.fori_loop(
+            0, 4 * (blocks4 - 1),
+            lambda idx, _: step4(idx // (blocks4 - 1), idx % (blocks4 - 1) + 1), 0, unroll=2,
+        )
+    for copy in early(p):
+        copy.wait()
     lax.fori_loop(0, rows // SPAN, step1, 0, unroll=2)
-
-
-def attend(mesh, group, behind, nat, res, res_halo, nat_halo):
+    for copy in late(p):
+        copy.wait()
+    lax.fori_loop(0, 4, lambda r, _: step4(r, 0), 0, unroll=2)
+    lax.fori_loop(0, WIDE * blocks16, step16, 0, unroll=2)
+    lax.fori_loop(0, rows // SPAN, merge, 0, unroll=2)
+
+
+def attend(mesh, group, behind, nat, res):
     rows, part3 = nat.shape
     part = part3 // 3
     pairs = part // LANES
@@ -329,42 +343,42 @@
     def res_spec(off):
         return pl.BlockSpec((WIDE, steps, LANES), lambda p: (0, 0, p + off))
 
-    def halo_spec(off):
-        return pl.BlockSpec((behind, WIDE, steps, LANES), lambda p: (0, 0, 0, p + off))
-
     f32 = jnp.float32
     state = pltpu.VMEM((rows, LANES), f32)
     return pl.pallas_call(
-        functools.partial(attend_kernel, group, behind),
+        functools.partial(attend_kernel, mesh.shape["sp"], group, behind, pairs),
         grid=(pairs,),
         out_shape=(
             jax.ShapeDtypeStruct((rows, part), jnp.bfloat16),
             jax.ShapeDtypeStruct((pairs, 2, rows), f32),
         ),
         in_specs=[
+            ANY, ANY,
             nat_spec(rows, 0), nat_spec(rows, pairs), nat_spec(rows, 2 * pairs),
             res_spec(0), res_spec(pairs), res_spec(2 * pairs),
-            halo_spec(0), halo_spec(pairs),
-            nat_spec(SPAN, 0), nat_spec(SPAN, pairs),
         ],
         out_specs=(
             pl.BlockSpec((rows, LANES), lambda p: (0, p)),
             pl.BlockSpec((1, 2, rows), lambda p: (p, 0, 0)),
         ),
         scratch_shapes=[
-            pltpu.VMEM((WIDE, SPAN + steps, LANES), jnp.bfloat16),
-            pltpu.VMEM((WIDE, SPAN + steps, LANES), jnp.bfloat16),
-            pltpu.VMEM((SPAN + rows, LANES), jnp.bfloat16),
-            pltpu.VMEM((SPAN + rows, LANES), jnp.bfloat16),
-            state, state, state, state, state, state,
+            pltpu.VMEM((pairs, WIDE, SPAN + steps, LANES), jnp.bfloat16),
+            pltpu.VMEM((pairs, WIDE, SPAN + steps, LANES), jnp.bfloat16),
+            pltpu.VMEM((pairs, SPAN + rows, LANES), jnp.bfloat16),
+            pltpu.VMEM((pairs, SPAN + rows, LANES), jnp.bfloat16),
+            state, state, state, state, state, state, state, state, state,
             pltpu.VMEM((2, SPAN, 2 * SPAN), f32),
             pltpu.VMEM((2, SPAN, 2 * SPAN), f32),
             pltpu.VMEM((2, block, block + SPAN), f32),
+            pltpu.SemaphoreType.DMA((pairs, 2 * behind + 2)),
+            pltpu.SemaphoreType.DMA((pairs, 2 * behind + 2)),
         ],
-        compiler_params=pltpu.CompilerParams(vmem_limit_bytes=56 * 1024 * 1024),
+        compiler_params=pltpu.CompilerParams(
+            vmem_limit_bytes=56 * 1024 * 1024, collective_id=1, has_side_effects=True
+        ),
         cost_estimate=pl.CostEstimate(flops=6 * rows * 512 * part, bytes_accessed=8 * rows * part, transcendentals=0),
         name="attend_windows",
-    )(nat, nat, nat, res, res, res, res_halo, res_halo, nat_halo, nat_halo)
+    )(nat, res, nat, nat, nat, res, res, res)
 
 
 def return_kernel(group, rows, att_ref, lw_ref, att_out, lw_out, send, recv, local):
@@ -474,8 +488,7 @@
     nat, res = project(
         hid.reshape(all_rows, depth), pre_gain[None, :], wq, wk, wv, cos_part, sin_part
     )
-    res_halo, nat_halo = halo(mesh, group, behind, nat, res)
-    att, lw = attend(mesh, group, behind, nat, res, res_halo, nat_halo)
+    att, lw = attend(mesh, group, behind, nat, res)
     attended, log_weight = give_back(mesh, group, att, lw)
     partial = jnp.dot(attended, out_proj, preferred_element_type=jnp.float32).astype(jnp.bfloat16)
     partial = partial.reshape(n_tp, rows // n_tp, depth)

time: 201 us -> 180 us (0.90)
  Pallas kernels: 178 us -> 157 us
    pallas_call x2 -> x1, Pallas kernels: 83.4 us -> 62.7 us  [attend(): pl.pallas_call(functools.partial(attend_kernel, mesh.shape['sp'], group,...]
where the time goes in v3:
time: 180 us; the launch traced here: 179 us
  Pallas kernels  157 us (87%)
  other arithmetic  9.98 us (6%)
  matrix products  6.19 us (3%)
  local copies, waits for them, and re-layouts  5.15 us (3%)
    pallas_call x1, Pallas kernels, gather(): pl.pallas_call(functools.partial(gather_kernel, n_sp, group), out_shape=(...  62.8 us
    pallas_call x1, Pallas kernels, attend(): pl.pallas_call(functools.partial(attend_kernel, mesh.shape['sp'], group,...  62.7 us
    pallas_call x1, Pallas kernels, project(): pl.pallas_call(functools.partial(project_kernel, part), grid=(rows // blo...  14.6 us
    pallas_call x1, Pallas kernels, give_back(): pl.pallas_call(functools.partial(return_kernel, group, rows), out_shape=(...  14.2 us
    dot_general x1, matrix products, body(): jnp.dot(attended, out_proj, preferred_element_type=jnp.float32)  6.19 us
    neg x1, other arithmetic, tables(): -sin_part  3.72 us

profile of v3, /device:TPU:0, one launch (start us, length us, event | category | flops | bytes accessed | tf_op | source)
XLA Modules:
  0.0 179.4 jit_solution(10043821680578424435)
XLA Ops:
  0.7 1.3 constant_dynamic-slice_fusion.wq_ref
  2.0 3.7 %fusion.3 = (f32[2048,32]{1,0:T(8,128)S(1)}, f32[2048,32]{1,0:T(8,128)S(1)}, f32[2048,32]{1,0:T(8,128)S(1)}) fusion(f32[32]{0:T(128)S(1)} %negate_power_fusion, f32[2048]{0:T(1024)S(1)} %add_convert_fusion), kind=kLoop, calls=%fused_computation.11 | loop fusion | flops 131072 | bytes 794752 | tf_op jit(solution)/shard_map/neg | solution.py:470
  5.7 3.0 %pad_maximum_fusion = (f32[2048,128]{1,0:T(8,128)}, f32[2048,128]{1,0:T(8,128)}) fusion(f32[2048,32]{1,0:T(8,128)S(1)} %get-tuple-element.22, f32[2048,32]{1,0:T(8,128)S(1)} %get-tuple-element.21, f32[2048,32]{1,0:T(8,128)S(1)} %get-tuple-element.20), kind=kLoop, calls=%fused_computation.9 | loop fusion | flops 1572864 | bytes 2883584 | tf_op jit(solution)/shard_map/concatenate | solution.py:469
  8.7 0.0 copy-start.2
  8.7 62.8 %gather_blocks.1 = (bf16[4,512,2048]{2,1,0:T(8,128)(2,1)}, bf16[2048,256]{1,0:T(8,128)(2,1)}, bf16[2048,256]{1,0:T(8,128)(2,1)}) custom-call(bf16[512,2048]{1,0:T(8,128)(2,1)} %hid_ref.1, bf16[128,1024]{1,0:T(8,128)(2,1)} %wk_ref.1, bf16[128,1024]{1,0:T(8,128)(2,1)} %wv_ref.1), custom_call_target="tpu_custom_call" | custom-call | tf_op jit(solution)/shard_map/gather_blocks/pallas_call | solution.py:105
  71.5 0.0 copy-done.2
  71.5 0.0 copy-start
  71.5 1.2 copy-done
  72.7 0.0 copy-start.1
  72.7 1.2 copy-done.1
  74.0 14.6 %project_rows.1 = (bf16[2048,768]{1,0:T(8,128)(2,1)}, bf16[16,128,768]{2,1,0:T(8,128)(2,1)}) custom-call(bf16[2048,2048]{1,0:T(8,128)(2,1)} %bitcast.18, f32[1,2048]{1,0:T(1,128)S(1)} %bitcast.14, bf16[2048,256]{1,0:T(8,128)(2,1)S(1)} %constant_dynamic-slice_fusion.wq_ref, bf16[2048,256]{1,0:T(8,128)(2,1)S(1)} %copy-done, bf16[2048,256]{1,0:T(8,128)(2,1)S(1)} %copy-done.1, ...), custom_call_target="tpu_custom_call" | custom-call | flops 6442450944 | bytes 8388608 | tf_op jit(solution)/shard_map/project_rows/pallas_call | solution.py:152
  88.6 62.7 %attend_windows.1 = (bf16[2048,256]{1,0:T(8,128)(2,1)}, f32[2,2,2048]{2,1,0:T(2,128)}) custom-call(bf16[2048,768]{1,0:T(8,128)(2,1)} %get-tuple-element.14.nat_ref.qn.kn.vn, bf16[16,128,768]{2,1,0:T(8,128)(2,1)} %get-tuple-element.15.res_ref.qr.kr.vr, bf16[2048,768]{1,0:T(8,128)(2,1)} %get-tuple-element.14.nat_ref.qn.kn.vn, ...), custom_call_target="tpu_custom_call" | custom-call | flops 1610612736 | bytes 4194304 | tf_op jit(solution)/shard_map/attend_windows/pallas_call | solution.py:348
  151.3 14.2 %give_back.1 = (bf16[512,1024]{1,0:T(8,128)(2,1)}, f32[4,2,2,512]{3,2,1,0:T(2,128)}) custom-call(bf16[2048,256]{1,0:T(8,128)(2,1)} %get-tuple-element.16.att_ref, f32[2,2,2048]{2,1,0:T(2,128)} %get-tuple-element.17.lw_ref), custom_call_target="tpu_custom_call" | custom-call | tf_op jit(solution)/shard_map/give_back/pallas_call | solution.py:416
  165.5 1.4 reshape.38
  166.9 6.2 %convolution_convert_fusion = bf16[512,2048]{1,0:T(8,128)(2,1)} fusion(bf16[512,1024]{1,0:T(8,128)(2,1)} %get-tuple-element.18, bf16[1024,2048]{1,0:T(8,128)(2,1)} %param.12), kind=kOutput, calls=%fused_computation | convolution fusion | flops 2148532224 | bytes 7340032 | tf_op jit(solution)/shard_map/dot_general | solution.py:493
  173.1 0.0 copy-start.4
  173.1 0.0 copy-start.5
  173.1 3.0 %swap_partials.1 = bf16[1,256,2048]{2,1,0:T(8,128)(2,1)} custom-call(bf16[2,256,2048]{2,1,0:T(8,128)(2,1)} %bitcast.15), custom_call_target="tpu_custom_call" | custom-call | tf_op jit(solution)/shard_map/swap_partials/pallas_call | solution.py:450
  176.2 0.0 copy-done.4
  176.2 0.0 copy-start.3
  176.2 1.7 fusion
  177.9 0.0 copy-done.5
  177.9 0.0 copy-done.3
  178.0 1.5 fusion.2
  (3 shorter events, 0.0 us)
Async XLA Ops:
  8.7 62.8 %copy-start.2 = (f32[2048]{0:T(1024)S(1)}, f32[2048]{0:T(1024)}, u32[]{:S(2)}) copy-start(f32[2048]{0:T(1024)} %param.8) | copy-start | bytes 24580
  71.5 1.2 copy-start
  72.7 1.2 copy-start.1
  173.1 3.1 %copy-start.4 = (bf16[512,2048]{1,0:T(8,128)(2,1)S(1)}, bf16[512,2048]{1,0:T(8,128)(2,1)}, u32[]{:S(2)}) copy-start(bf16[512,2048]{1,0:T(8,128)(2,1)} %convolution_convert_fusion) | copy-start | bytes 6291460
  173.1 4.8 %copy-start.5 = (f32[2048]{0:T(1024)S(1)}, f32[2048]{0:T(1024)}, u32[]{:S(2)}) copy-start(f32[2048]{0:T(1024)} %param.13) | copy-start | bytes 24580
  176.2 1.8 copy-start.3
